TPU v7x, 32 devices: a whole 2x2x4 slice. The times are simulated.
32 devices in a mesh: ep: 8 (over z, x), tp: 4 (over y, core).
Axes of the slice: x: 2, y: 2, z: 4, core: 2. Of those that a mesh axis runs over, the one named last changes fastest.
Arguments:
- residual: bfloat16 [1024, 2048], P('ep', 'tp'), may hold values from -61 to 61
- in_gain: float32 [2048], replicated, may hold values from 0.1 to 1.9
- in_weight: bfloat16 [2048, 1024], P(None, 'tp'), may hold values from -0.125 to 0.125
- state: float32 [2, 1024, 4096], P(None, 'ep', 'tp'), may hold values from -3 to 3
- decay_rate: float32 [64, 64], P('tp'), may hold values from 0.1 to 1
- frequency: float32 [64, 64], P('tp'), may hold values from 0 to 200
- log_step: float32 [64], P('tp'), may hold values from -3 to -0.7
- in_coef: float32 [2, 64, 64, 16], P(None, 'tp'), may hold values from -1 to 1
- out_coef: float32 [2, 64, 16, 64], P(None, 'tp'), may hold values from -0.75 to 0.75
- skip_gain: float32 [1024], P('tp'), may hold values from -3 to 3
- out_weight: bfloat16 [1024, 2048], replicated, may hold values from -0.1875 to 0.1875
- mid_gain: float32 [2048], replicated, may hold values from 0.1 to 1.9
- gate_vector: bfloat16 [2048], replicated, may hold values from -0.125 to 0.125
- routes: int32 [1024, 4], P('ep'), may hold values from 0 to 31, all different within a row; in each aligned block of 128 rows (0 to 127, 128 to 255, ...) at most 32 rows name the same one
- route_weight: float32 [1024, 4], P('ep'), may hold values from 0.1 to 1
- expert_gate: bfloat16 [32, 2048, 512], P(('ep', 'tp')), may hold values from -0.125 to 0.125
- expert_up: bfloat16 [32, 2048, 512], P(('ep', 'tp')), may hold values from -0.125 to 0.125
- expert_down: bfloat16 [32, 512, 2048], P(('ep', 'tp')), may hold values from -0.25 to 0.25
- shared_gate: bfloat16 [2048, 4096], P(None, 'ep'), may hold values from -0.125 to 0.125
- shared_up: bfloat16 [2048, 4096], P(None, 'ep'), may hold values from -0.125 to 0.125
- shared_down: bfloat16 [4096, 2048], P('ep'), may hold values from -0.09375 to 0.09375
Outputs:
- layer_out: bfloat16 [1024, 2048], P(('ep', 'tp'))
- new_state: float32 [2, 1024, 4096], P(None, 'ep', 'tp')
Inputs may be any that keep to these rules, and one draw needn't show every extreme that they name: `routes`: each row names 4 different experts. Among the rows of one index of ep no expert is named more than 32 times, a bound that some block reaches.
All inputs are finite; a program needn't handle non-finite values.
Results may differ from a plain program's by a relative error of at most 0.0085.
Values may be sent and summed in bfloat16 or wider, within the bound.
A program may use at most 128 MiB of HBM per device.

v0:
```python
import jax
import jax.numpy as jnp
from jax import lax
from jax.sharding import PartitionSpec as P

norm_eps = 1e-05
routed_scale = 2.5


def layer_norm(values, gain_vec):
    row_mean = jnp.mean(values, axis=-1, keepdims=True)
    row_square = jnp.mean(values * values, axis=-1, keepdims=True)
    return (values - row_mean) * lax.rsqrt(row_square - row_mean * row_mean + norm_eps) * gain_vec


def coefficients(decay_rate, frequency, log_step, in_coef):
    time_step = jnp.exp(log_step)[:, None]
    real_rate = -decay_rate
    magnitude = jnp.exp(real_rate * time_step)
    keep_re = magnitude * jnp.cos(frequency * time_step)
    keep_im = magnitude * jnp.sin(frequency * time_step)
    denominator = real_rate * real_rate + frequency * frequency
    factor_re = ((keep_re - 1.0) * real_rate + keep_im * frequency) / denominator
    factor_im = (keep_im * real_rate - (keep_re - 1.0) * frequency) / denominator
    push_re = factor_re[..., None] * in_coef[0] - factor_im[..., None] * in_coef[1]
    push_im = factor_re[..., None] * in_coef[1] + factor_im[..., None] * in_coef[0]
    return (keep_re, keep_im, push_re, push_im)


def mixer_step(
    normed, in_weight, state, decay_rate, frequency, log_step, in_coef, out_coef, skip_gain
):
    row_count = normed.shape[0]
    group_count, state_count = decay_rate.shape
    keep_re, keep_im, push_re, push_im = coefficients(decay_rate, frequency, log_step, in_coef)
    drive = jnp.dot(normed, in_weight, preferred_element_type=jnp.float32).astype(jnp.bfloat16)
    drive_f = drive.astype(jnp.float32).reshape(row_count, group_count, -1)
    highest = lax.Precision.HIGHEST
    input_re = jnp.einsum("tgh,gph->tgp", drive_f, push_re, precision=highest)
    input_im = jnp.einsum("tgh,gph->tgp", drive_f, push_im, precision=highest)
    old_re = state[0].reshape(row_count, group_count, state_count)
    old_im = state[1].reshape(row_count, group_count, state_count)
    new_re = keep_re * old_re - keep_im * old_im + input_re
    new_im = keep_re * old_im + keep_im * old_re + input_im
    read_out = jnp.einsum("ghp,tgp->tgh", out_coef[0], new_re, precision=highest) - jnp.einsum(
        "ghp,tgp->tgh", out_coef[1], new_im, precision=highest
    )
    read_out = read_out.reshape(row_count, -1) + skip_gain * drive_f.reshape(row_count, -1)
    mixed_rows = jax.nn.gelu(read_out, approximate=True).astype(jnp.bfloat16)
    updated = jnp.stack([new_re.reshape(row_count, -1), new_im.reshape(row_count, -1)])
    return (mixed_rows, updated)


def route_slots(routes, experts):
    flat_routes = routes.reshape(-1)
    onehot = (flat_routes[:, None] == jnp.arange(experts, dtype=jnp.int32)[None, :]).astype(
        jnp.int32
    )
    before = jnp.cumsum(onehot, axis=0) - onehot
    return jnp.sum(before * onehot, axis=1).reshape(routes.shape)


def expert_block(row_block, gate_weight, up_weight, down_weight):
    gate_part = jnp.dot(row_block, gate_weight, preferred_element_type=jnp.float32)
    up_part = jnp.dot(row_block, up_weight, preferred_element_type=jnp.float32)
    hidden = (jax.nn.silu(gate_part) * up_part).astype(jnp.bfloat16)
    return jnp.dot(hidden, down_weight, preferred_element_type=jnp.float32).astype(jnp.bfloat16)


def per_device(
    residual,
    in_gain,
    in_weight,
    state,
    decay_rate,
    frequency,
    log_step,
    in_coef,
    out_coef,
    skip_gain,
    out_weight,
    mid_gain,
    gate_vector,
    routes,
    route_weight,
    expert_gate,
    expert_up,
    expert_down,
    shared_gate,
    shared_up,
    shared_down,
):
    tp_count = lax.axis_size("tp")
    ep_count = lax.axis_size("ep")
    tp_place = lax.axis_index("tp")
    seq_rows, feat_part = residual.shape
    width = feat_part * tp_count
    own_values = residual.astype(jnp.float32)
    row_total, row_squares = lax.psum(
        (jnp.sum(own_values, axis=1), jnp.sum(own_values * own_values, axis=1)), "tp"
    )
    row_mean = row_total / width
    row_scale = lax.rsqrt(row_squares / width - row_mean * row_mean + norm_eps)
    gain_part = lax.dynamic_slice_in_dim(in_gain, tp_place * feat_part, feat_part, 0)
    normed_part = ((own_values - row_mean[:, None]) * row_scale[:, None] * gain_part).astype(
        jnp.bfloat16
    )
    normed, full_resid = (
        lax.all_gather(normed_part, "tp", axis=1, tiled=True),
        lax.all_gather(residual, "tp", axis=1, tiled=True),
    )
    mixed_part, new_state = mixer_step(
        normed, in_weight, state, decay_rate, frequency, log_step, in_coef, out_coef, skip_gain
    )
    mixed_rows = lax.all_gather(mixed_part, "tp", axis=1, tiled=True)
    after_mix = full_resid.astype(jnp.float32) + jnp.dot(
        mixed_rows, out_weight, preferred_element_type=jnp.float32
    )
    normed_mid = layer_norm(after_mix, mid_gain).astype(jnp.bfloat16)
    per_dev = seq_rows // tp_count
    own_mid = lax.dynamic_slice_in_dim(normed_mid, tp_place * per_dev, per_dev, 0)
    own_after = lax.dynamic_slice_in_dim(after_mix, tp_place * per_dev, per_dev, 0)
    experts = ep_count * tp_count
    top_count = routes.shape[1]
    capacity = max(2, 2 * seq_rows * top_count // experts)
    slot_rank = route_slots(routes, experts)
    dest_tp = routes % tp_count
    dest_ep = routes // tp_count
    is_mine = dest_tp == tp_place
    slot_place = dest_ep * capacity + slot_rank
    slot_total = ep_count * capacity
    matches = (
        slot_place.reshape(-1)[None, :] == jnp.arange(slot_total, dtype=jnp.int32)[:, None]
    ) & is_mine.reshape(-1)[None, :]
    token_ids = jnp.repeat(jnp.arange(seq_rows, dtype=jnp.int32), top_count)
    slot_token = jnp.sum(jnp.where(matches, token_ids[None, :], 0), axis=1)
    outgoing = normed_mid[slot_token].reshape(ep_count, capacity, width)
    copies = jnp.broadcast_to(own_mid[None], (ep_count, per_dev, width))
    got_slots, got_rows = (
        lax.all_to_all(outgoing, "ep", split_axis=0, concat_axis=0, tiled=True),
        lax.all_to_all(copies, "ep", split_axis=0, concat_axis=0, tiled=True),
    )
    flat_rows = got_slots.reshape(-1, width)
    result = expert_block(flat_rows, expert_gate[0], expert_up[0], expert_down[0])
    computed = result.reshape(got_slots.shape)
    returned = lax.all_to_all(computed, "ep", split_axis=0, concat_axis=0, tiled=True)
    piece = got_rows.reshape(-1, width)
    gate_part = jnp.dot(piece, shared_gate, preferred_element_type=jnp.float32)
    up_part = jnp.dot(piece, shared_up, preferred_element_type=jnp.float32)
    shared_hidden = (jax.nn.silu(gate_part) * up_part).astype(jnp.bfloat16)
    partial_rows = jnp.dot(shared_hidden, shared_down, preferred_element_type=jnp.float32)
    partial_back = lax.all_to_all(
        partial_rows.reshape(ep_count, per_dev, width).astype(jnp.bfloat16),
        "ep",
        split_axis=0,
        concat_axis=0,
        tiled=True,
    ).astype(jnp.float32)
    shared = jnp.sum(partial_back, axis=0)
    flat_back = returned.reshape(slot_total, width)
    weights = route_weight / jnp.sum(route_weight, axis=-1, keepdims=True) * routed_scale
    picked = flat_back[jnp.where(is_mine, slot_place, 0)].astype(jnp.float32)
    routed_part = jnp.sum(jnp.where(is_mine, weights, 0.0)[..., None] * picked, axis=1)
    routed = lax.psum_scatter(
        routed_part.astype(jnp.bfloat16), "tp", scatter_dimension=0, tiled=True
    ).astype(jnp.float32)
    gate_value = jax.nn.sigmoid(jnp.dot(own_mid, gate_vector, preferred_element_type=jnp.float32))
    layer_out = (own_after + routed + gate_value[:, None] * shared).astype(jnp.bfloat16)
    return (layer_out, new_state)


def solution(mesh):
    return jax.shard_map(
        per_device,
        mesh=mesh,
        in_specs=(
            P("ep", "tp"),
            P(),
            P(None, "tp"),
            P(None, "ep", "tp"),
            P("tp", None),
            P("tp", None),
            P("tp"),
            P(None, "tp", None, None),
            P(None, "tp", None, None),
            P("tp"),
            P(),
            P(),
            P(),
            P("ep", None),
            P("ep", None),
            P(("ep", "tp"), None, None),
            P(("ep", "tp"), None, None),
            P(("ep", "tp"), None, None),
            P(None, "ep"),
            P(None, "ep"),
            P("ep", None),
        ),
        out_specs=(P(("ep", "tp"), None), P(None, "ep", "tp")),
        check_vma=False,
    )
```

profile of v0, /device:TPU:0, one launch (start us, length us, event | category | flops | bytes accessed | tf_op | source)
XLA Modules:
  0.0 208.7 jit_solution(2249695286340410470)
XLA Ops:
  7.2 0.9 copy.74
  8.1 0.7 eq.54
  8.9 1.0 convert_reduce_fusion.1
  9.9 10.3 %all_gather.9 = bf16[128,2048]{1,0:T(8,128)(2,1)} all-gather(bf16[128,512]{1,0:T(8,128)(2,1)} %param.21), channel_id=1, replica_groups=mesh['ep'=8,'tp'=4] {'tp'}, dimensions={1}, use_global_device_ids=true | all-gather | bytes 655360 | tf_op jit(solution)/shard_map/all_gather | solution.py:110
  20.2 1.3 exp.16
  21.4 6.0 %all-reduce = (f32[128]{0:T(128)S(1)}, f32[128]{0:T(128)S(1)}) all-reduce(f32[128]{0:T(128)S(1)} %get-tuple-element.5, f32[128]{0:T(128)S(1)} %get-tuple-element.4), channel_id=1, replica_groups=mesh['ep'=8,'tp'=4] {'tp'}, use_global_device_ids=true, to_apply=%region_3.0 | all-reduce | flops 256 | bytes 2048 | tf_op jit(solution)/shard_map/psum | solution.py:99
  27.4 0.8 dynamic_slice.9
  28.2 1.0 fusion.33
  29.2 7.3 %all_gather.10 = bf16[128,2048]{1,0:T(8,128)(2,1)S(1)} all-gather(bf16[128,512]{1,0:T(8,128)(2,1)S(1)} %fusion.33), channel_id=1, replica_groups=mesh['ep'=8,'tp'=4] {'tp'}, dimensions={1}, use_global_device_ids=true | all-gather | bytes 655360 | tf_op jit(solution)/shard_map/all_gather | solution.py:109
  36.5 1.5 convolution_convert_fusion.2
  38.2 2.1 %fusion.75 = (f32[1,128,1024]{2,1,0:T(8,128)S(1)}, f32[1,128,1024]{2,1,0:T(8,128)}) fusion(f32[2,128,1024]{2,1,0:T(8,128)} %param.24), kind=kLoop, calls=%fused_computation.120 | loop fusion | bytes 2097152 | tf_op jit(solution)/shard_map/slice | solution.py:41
  40.5 1.2 copy.70
  41.8 0.8 add_divide_fusion
  42.7 1.6 fusion.8
  44.2 1.6 fusion.9
  45.8 0.8 reduce_sum.85
  46.9 1.2 reduce-window.6
  48.1 0.2 slice_reduce_fusion
  49.2 1.6 fusion.46
  50.8 1.6 convolution_subtract_fusion
  52.7 5.9 %all_gather.11 = bf16[128,1024]{1,0:T(8,128)(2,1)S(1)} all-gather(bf16[128,256]{1,0:T(8,128)(2,1)S(1)} %fusion.44), channel_id=1, replica_groups=mesh['ep'=8,'tp'=4] {'tp'}, dimensions={1}, use_global_device_ids=true | all-gather | bytes 327680 | tf_op jit(solution)/shard_map/all_gather | solution.py:115
  58.5 3.1 %fusion.72 = (f32[128]{0:T(128)S(1)}, f32[128]{0:T(128)S(1)}, f32[128,2048]{1,0:T(8,128)S(1)}) fusion(bf16[128,1024]{1,0:T(8,128)(2,1)S(1)} %all_gather.11, bf16[1024,2048]{1,0:T(8,128)(2,1)} %param.31, bf16[128,2048]{1,0:T(8,128)(2,1)S(1)} %copy-done.4), kind=kOutput, calls=%fused_computation.119 | convolution fusion | flops 538181376 | bytes 6030336 | tf_op jit(solution)/shard_map/dot_general | solution.py:116
  61.7 1.0 copy-done.1
  62.7 0.2 multiply_convert_fusion
  62.9 2.3 %gather_fusion = bf16[256,2048]{1,0:T(8,128)(2,1)} fusion(bf16[128,2048]{1,0:T(8,128)(2,1)S(1)} %multiply_convert_fusion, s32[1024]{0:T(1024)S(1)} %pad_clamp_fusion.1), kind=kCustom, calls=%fused_computation | custom fusion | bytes 2098176 | tf_op jit(solution)/shard_map/gather | solution.py:137
  65.2 5.8 %all-to-all-start = ((bf16[8,32,2048]{2,1,0:T(8,128)(2,1)}), bf16[8,32,2048]{2,1,0:T(8,128)(2,1)}, u32[]{:S(2)}, u32[]{:S(2)}) async-start(bf16[8,32,2048]{2,1,0:T(8,128)(2,1)} %bitcast.116), calls=%async_computation | async-start | bytes 2097152 | tf_op jit(solution)/shard_map/all_to_all | solution.py:140
  71.0 26.4 %all-to-all-done = bf16[8,32,2048]{2,1,0:T(8,128)(2,1)} async-done(((bf16[8,32,2048]{2,1,0:T(8,128)(2,1)}), bf16[8,32,2048]{2,1,0:T(8,128)(2,1)}, u32[]{:S(2)}, u32[]{:S(2)}) %all-to-all-start) | async-done | bytes 1048608 | tf_op jit(solution)/shard_map/all_to_all | solution.py:140
  97.4 1.1 broadcast_in_dim.30
  98.5 3.6 %all-to-all-start.2 = ((bf16[8,32,2048]{2,1,0:T(8,128)(2,1)}), bf16[8,32,2048]{2,1,0:T(8,128)(2,1)S(1)}, u32[]{:S(2)}, u32[]{:S(2)}) async-start(bf16[8,32,2048]{2,1,0:T(8,128)(2,1)} %broadcast_in_dim.30), calls=%async_computation.3 | async-start | bytes 2097152 | tf_op jit(solution)/shard_map/all_to_all | solution.py:141
  102.1 3.4 %fusion.3 = f32[256,512]{1,0:T(8,128)} fusion(bf16[256,2048]{1,0:T(8,128)(2,1)} %bitcast.15, bf16[1,2048,512]{2,1,0:T(8,128)(2,1)} %param.36), kind=kOutput, calls=%fused_computation.9 | convolution fusion | flops 536870912 | bytes 3670016 | tf_op jit(solution)/shard_map/dot_general | solution.py:64
  105.5 4.3 %convolution_convert_fusion.1 = bf16[256,2048]{1,0:T(8,128)(2,1)} fusion(bf16[1,512,2048]{2,1,0:T(8,128)(2,1)S(1)} %copy-done, bf16[256,2048]{1,0:T(8,128)(2,1)} %bitcast.15, bf16[1,2048,512]{2,1,0:T(8,128)(2,1)} %param.37, f32[256,512]{1,0:T(8,128)} %fusion.3), kind=kOutput, calls=%fused_computation.4 | convolution fusion | flops 1075052544 | bytes 6815744 | tf_op jit(solution)/shard_map/dot_general | solution.py:67
  109.9 18.2 %all-to-all-done.2 = bf16[8,32,2048]{2,1,0:T(8,128)(2,1)S(1)} async-done(((bf16[8,32,2048]{2,1,0:T(8,128)(2,1)}), bf16[8,32,2048]{2,1,0:T(8,128)(2,1)S(1)}, u32[]{:S(2)}, u32[]{:S(2)}) %all-to-all-start.2) | async-done | bytes 1048608 | tf_op jit(solution)/shard_map/all_to_all | solution.py:141
  128.1 1.0 copy-done.5
  129.1 3.6 %all-to-all-start.1 = ((bf16[8,32,2048]{2,1,0:T(8,128)(2,1)}), bf16[8,32,2048]{2,1,0:T(8,128)(2,1)S(1)}, u32[]{:S(2)}, u32[]{:S(2)}) async-start(bf16[8,32,2048]{2,1,0:T(8,128)(2,1)} %bitcast.120), calls=%async_computation.1 | async-start | bytes 2097152 | tf_op jit(solution)/shard_map/all_to_all | solution.py:146
  132.7 3.5 %fusion.76 = f32[256,512]{1,0:T(8,128)} fusion(bf16[256,2048]{1,0:T(8,128)(2,1)} %bitcast.118, bf16[2048,512]{1,0:T(8,128)(2,1)} %param.39), kind=kOutput, calls=%fused_computation.121 | convolution fusion | flops 536870912 | bytes 3670016 | tf_op jit(solution)/shard_map/dot_general | solution.py:148
  136.2 5.0 %convolution_convert_fusion = bf16[256,2048]{1,0:T(8,128)(2,1)} fusion(bf16[512,2048]{1,0:T(8,128)(2,1)} %param.41, bf16[256,2048]{1,0:T(8,128)(2,1)} %bitcast.119, bf16[2048,512]{1,0:T(8,128)(2,1)} %param.40, f32[256,512]{1,0:T(8,128)} %fusion.76), kind=kOutput, calls=%fused_computation.3 | convolution fusion | flops 1075052544 | bytes 6815744 | tf_op jit(solution)/shard_map/dot_general | solution.py:151
  141.2 17.5 %all-to-all-done.1 = bf16[8,32,2048]{2,1,0:T(8,128)(2,1)S(1)} async-done(((bf16[8,32,2048]{2,1,0:T(8,128)(2,1)}), bf16[8,32,2048]{2,1,0:T(8,128)(2,1)S(1)}, u32[]{:S(2)}, u32[]{:S(2)}) %all-to-all-start.1) | async-done | bytes 1048608 | tf_op jit(solution)/shard_map/all_to_all | solution.py:146
  158.6 4.2 %all-to-all-start.3 = ((bf16[8,32,2048]{2,1,0:T(8,128)(2,1)}), bf16[8,32,2048]{2,1,0:T(8,128)(2,1)}, u32[]{:S(2)}, u32[]{:S(2)}) async-start(bf16[8,32,2048]{2,1,0:T(8,128)(2,1)} %bitcast.117), calls=%async_computation.4 | async-start | bytes 2097152 | tf_op jit(solution)/shard_map/all_to_all | solution.py:152
  162.9 0.2 reduce-scatter.2.cloned.1.call-start
  163.5 3.3 %gather_fusion.1 = bf16[512,2048]{1,0:T(8,128)(2,1)} fusion(bf16[256,2048]{1,0:T(8,128)(2,1)S(1)} %bitcast.109, s32[1024]{0:T(1024)S(1)} %pad_clamp_fusion), kind=kCustom, calls=%fused_computation.1 | custom fusion | bytes 4196352 | tf_op jit(solution)/shard_map/gather | solution.py:162
  166.8 4.8 %reshape.122 = f32[128,4,2048]{2,1,0:T(4,128)} reshape(bf16[512,2048]{1,0:T(8,128)(2,1)} %gather_fusion.1) | data formatting | bytes 6291456 | tf_op jit(solution)/shard_map/convert_element_type | solution.py:162
  171.6 6.3 %multiply_reduce_fusion = bf16[128,2048]{1,0:T(8,128)(2,1)} fusion(f32[128,4,2048]{2,1,0:T(4,128)} %reshape.122, f32[128,4]{1,0:T(8,128)S(1)} %copy.73), kind=kLoop, calls=%fused_computation.2 | loop fusion | flops 1835008 | bytes 4720640 | tf_op jit(solution)/shard_map/reduce_sum | solution.py:163
  177.9 1.0 copy.82
  179.1 2.1 %pad_maximum_fusion = f32[2,128,1024]{2,1,0:T(8,128)} fusion(f32[1,128,1024]{2,1,0:T(8,128)} %copy.82, f32[1,128,1024]{2,1,0:T(8,128)S(1)} %copy.81), kind=kLoop, calls=%fused_computation.27 | loop fusion | flops 262144 | bytes 2097152 | tf_op jit(solution)/shard_map/stack | solution.py:50
  181.4 7.1 %all-to-all-done.3 = bf16[8,32,2048]{2,1,0:T(8,128)(2,1)} async-done(((bf16[8,32,2048]{2,1,0:T(8,128)(2,1)}), bf16[8,32,2048]{2,1,0:T(8,128)(2,1)}, u32[]{:S(2)}, u32[]{:S(2)}) %all-to-all-start.3) | async-done | bytes 1048608 | tf_op jit(solution)/shard_map/all_to_all | solution.py:152
  188.5 1.4 convert_reduce_fusion
  189.9 10.2 %reduce-scatter.2.cloned.1.call-done = bf16[32,2048]{1,0:T(8,128)(2,1)} async-done(((bf16[128,2048]{1,0:T(8,128)(2,1)}), bf16[32,2048]{1,0:T(8,128)(2,1)}) %reduce-scatter.2.cloned.1.call-update) | async-done | bytes 131088 | tf_op jit(solution)/shard_map/reduce_scatter | solution.py:164
  200.1 1.8 add_convert_fusion
  (59 shorter events, 2.5 us)
Async XLA Ops:
  7.2 98.4 %copy-start = (bf16[1,512,2048]{2,1,0:T(8,128)(2,1)S(1)}, bf16[1,512,2048]{2,1,0:T(8,128)(2,1)}, u32[]{:S(2)}) copy-start(bf16[1,512,2048]{2,1,0:T(8,128)(2,1)} %param.38) | copy-start | bytes 6291460
  38.2 3.6 %copy-start.9 = (f32[16,64]{1,0:T(8,128)S(1)}, f32[16,64]{1,0:T(8,128)}, u32[]{:S(2)}) copy-start(f32[16,64]{1,0:T(8,128)} %param.26) | copy-start | bytes 12292
  38.2 4.5 %copy-start.6 = (f32[2,16,64,16]{2,3,1,0:T(8,128)S(1)}, f32[2,16,64,16]{2,3,1,0:T(8,128)}, u32[]{:S(2)}) copy-start(f32[2,16,64,16]{2,3,1,0:T(8,128)} %param.28) | copy-start | bytes 393220
  41.8 4.8 %copy-start.7 = (s32[128,4]{0,1:T(4,128)S(1)}, s32[128,4]{0,1:T(4,128)}, u32[]{:S(2)}) copy-start(s32[128,4]{0,1:T(4,128)} %param.34) | copy-start | bytes 6148
  42.6 4.0 %copy-start.11 = (f32[128,4]{0,1:T(4,128)S(1)}, f32[128,4]{0,1:T(4,128)}, u32[]{:S(2)}) copy-start(f32[128,4]{0,1:T(4,128)} %param.35) | copy-start | bytes 6148
  42.6 4.2 %copy-start.10 = (s32[4,128]{1,0:T(4,128)S(1)}, s32[4,128]{1,0:T(4,128)}, u32[]{:S(2)}) copy-start(s32[4,128]{1,0:T(4,128)} %eq.54) | copy-start | bytes 6148
  45.8 6.8 %copy-start.13 = (f32[256]{0:T(256)S(1)}, f32[256]{0:T(256)}, u32[]{:S(2)}) copy-start(f32[256]{0:T(256)} %param.30) | copy-start | bytes 3076
  45.8 12.7 %copy-start.4 = (bf16[128,2048]{1,0:T(8,128)(2,1)S(1)}, bf16[128,2048]{1,0:T(8,128)(2,1)}, u32[]{:S(2)}) copy-start(bf16[128,2048]{1,0:T(8,128)(2,1)} %all_gather.9) | copy-start | bytes 1572868
  58.5 4.2 %copy-start.8 = (f32[2048]{0:T(1024)S(1)}, f32[2048]{0:T(1024)}, u32[]{:S(2)}) copy-start(f32[2048]{0:T(1024)} %param.32) | copy-start | bytes 24580
  61.7 1.0 copy-start.1
  65.2 32.2 %all-to-all-start = ((bf16[8,32,2048]{2,1,0:T(8,128)(2,1)}), bf16[8,32,2048]{2,1,0:T(8,128)(2,1)}, u32[]{:S(2)}, u32[]{:S(2)}) async-start(bf16[8,32,2048]{2,1,0:T(8,128)(2,1)} %bitcast.116), calls=%async_computation | async-start | bytes 2097152 | tf_op jit(solution)/shard_map/all_to_all | solution.py:140
  98.5 29.6 %all-to-all-start.2 = ((bf16[8,32,2048]{2,1,0:T(8,128)(2,1)}), bf16[8,32,2048]{2,1,0:T(8,128)(2,1)S(1)}, u32[]{:S(2)}, u32[]{:S(2)}) async-start(bf16[8,32,2048]{2,1,0:T(8,128)(2,1)} %broadcast_in_dim.30), calls=%async_computation.3 | async-start | bytes 2097152 | tf_op jit(solution)/shard_map/all_to_all | solution.py:141
  128.1 1.0 copy-start.5
  129.1 29.6 %all-to-all-start.1 = ((bf16[8,32,2048]{2,1,0:T(8,128)(2,1)}), bf16[8,32,2048]{2,1,0:T(8,128)(2,1)S(1)}, u32[]{:S(2)}, u32[]{:S(2)}) async-start(bf16[8,32,2048]{2,1,0:T(8,128)(2,1)} %bitcast.120), calls=%async_computation.1 | async-start | bytes 2097152 | tf_op jit(solution)/shard_map/all_to_all | solution.py:146
  158.6 29.8 %all-to-all-start.3 = ((bf16[8,32,2048]{2,1,0:T(8,128)(2,1)}), bf16[8,32,2048]{2,1,0:T(8,128)(2,1)}, u32[]{:S(2)}, u32[]{:S(2)}) async-start(bf16[8,32,2048]{2,1,0:T(8,128)(2,1)} %bitcast.117), calls=%async_computation.4 | async-start | bytes 2097152 | tf_op jit(solution)/shard_map/all_to_all | solution.py:152
  162.9 37.2 %reduce-scatter.2.cloned.1.call-start = ((), (), s32[]{:S(2)}) async-start(), calls=%async_computation.5 | async-start | bytes 655360 | tf_op jit(solution)/shard_map/reduce_scatter | solution.py:164
  171.6 6.3 %copy-start.12 = (bf16[2048]{0:T(1024)(128)(2,1)S(1)}, bf16[2048]{0:T(1024)(128)(2,1)}, u32[]{:S(2)}) copy-start(bf16[2048]{0:T(1024)(128)(2,1)} %param.33) | copy-start | bytes 12292
  171.6 6.3 %copy-start.3 = (f32[128,16,64]{0,2,1:T(8,128)S(1)}, f32[128,16,64]{0,2,1:T(8,128)}, u32[]{:S(2)}) copy-start(f32[128,16,64]{0,2,1:T(8,128)} %fusion.8) | copy-start | bytes 1572868
  171.6 7.4 %copy-start.2 = (f32[128,16,64]{0,2,1:T(8,128)S(1)}, f32[128,16,64]{0,2,1:T(8,128)}, u32[]{:S(2)}) copy-start(f32[128,16,64]{0,2,1:T(8,128)} %fusion.9) | copy-start | bytes 1572868
Sparse Core Ops, SparseCore 0:
  178.0 22.0 reduce-scatter.1
where the time goes:
time: 210 us; the launch traced here: 209 us
  waiting for transfers between devices  79.4 us (38%)
  blocking collectives  29.4 us (14%)
  matrix products  27.5 us (13%)
  local copies, waits for them, and re-layouts  23.6 us (11%)
  starting transfers between devices  17.5 us (8%)
  other arithmetic  17 us (8%)
  between operations  14.3 us (7%)
    all_to_all x1, waiting for transfers between devices, per_device(): lax.all_to_all(outgoing, 'ep', split_axis=0, concat_axis=0, tiled=True)  26.4 us
    all_to_all x1, waiting for transfers between devices, per_device(): lax.all_to_all(copies, 'ep', split_axis=0, concat_axis=0, tiled=True)  18.2 us
    all_to_all x1, waiting for transfers between devices, per_device(): lax.all_to_all(computed, 'ep', split_axis=0, concat_axis=0, tiled=True)  17.5 us
    all_gather x1, blocking collectives, per_device(): lax.all_gather(residual, 'tp', axis=1, tiled=True)  10.3 us
    reduce_scatter x1, waiting for transfers between devices, per_device(): lax.psum_scatter(routed_part.astype(jnp.bfloat16), 'tp', scatter_dimensio...  10.2 us
    all_gather x1, blocking collectives, per_device(): lax.all_gather(normed_part, 'tp', axis=1, tiled=True)  7.31 us
    all_to_all x1, waiting for transfers between devices, per_device(): lax.all_to_all(partial_rows.reshape(ep_count, per_dev, width).astype(jnp....  7.11 us
    reduce_sum x1, other arithmetic, per_device(): jnp.sum(jnp.where(is_mine, weights, 0.0)[..., None] * picked, axis=1)  6.28 us
  transfers between devices with their start and end apart: 5, of which 5 were waited for; matrix products, arithmetic and copies ran while one was open for 17% of the time, Pallas kernels for 0%

commit v1 on v0

v1 whole, which is shorter than its diff:
```python
import functools
import itertools

import jax
import jax.numpy as jnp
from jax import lax
from jax.experimental import pallas as pl
from jax.experimental.pallas import tpu as pltpu
from jax.sharding import PartitionSpec as P

norm_eps = 1e-05
routed_scale = 2.5
lanes = 128


def layer_norm(values, gain_vec):
    row_mean = jnp.mean(values, axis=-1, keepdims=True)
    row_square = jnp.mean(values * values, axis=-1, keepdims=True)
    return (values - row_mean) * lax.rsqrt(row_square - row_mean * row_mean + norm_eps) * gain_vec


def coefficients(decay_rate, frequency, log_step, in_coef):
    time_step = jnp.exp(log_step)[:, None]
    real_rate = -decay_rate
    magnitude = jnp.exp(real_rate * time_step)
    keep_re = magnitude * jnp.cos(frequency * time_step)
    keep_im = magnitude * jnp.sin(frequency * time_step)
    denominator = real_rate * real_rate + frequency * frequency
    factor_re = ((keep_re - 1.0) * real_rate + keep_im * frequency) / denominator
    factor_im = (keep_im * real_rate - (keep_re - 1.0) * frequency) / denominator
    push_re = factor_re[..., None] * in_coef[0] - factor_im[..., None] * in_coef[1]
    push_im = factor_re[..., None] * in_coef[1] + factor_im[..., None] * in_coef[0]
    return (keep_re, keep_im, push_re, push_im)


def mixer_step(
    normed, in_weight, state, decay_rate, frequency, log_step, in_coef, out_coef, skip_gain
):
    row_count = normed.shape[0]
    group_count, state_count = decay_rate.shape
    keep_re, keep_im, push_re, push_im = coefficients(decay_rate, frequency, log_step, in_coef)
    drive = jnp.dot(normed, in_weight, preferred_element_type=jnp.float32).astype(jnp.bfloat16)
    drive_f = drive.astype(jnp.float32).reshape(row_count, group_count, -1)
    highest = lax.Precision.HIGHEST
    input_re = jnp.einsum("tgh,gph->tgp", drive_f, push_re, precision=highest)
    input_im = jnp.einsum("tgh,gph->tgp", drive_f, push_im, precision=highest)
    old_re = state[0].reshape(row_count, group_count, state_count)
    old_im = state[1].reshape(row_count, group_count, state_count)
    new_re = keep_re * old_re - keep_im * old_im + input_re
    new_im = keep_re * old_im + keep_im * old_re + input_im
    read_out = jnp.einsum("ghp,tgp->tgh", out_coef[0], new_re, precision=highest) - jnp.einsum(
        "ghp,tgp->tgh", out_coef[1], new_im, precision=highest
    )
    read_out = read_out.reshape(row_count, -1) + skip_gain * drive_f.reshape(row_count, -1)
    mixed_rows = jax.nn.gelu(read_out, approximate=True).astype(jnp.bfloat16)
    updated = jnp.stack([new_re.reshape(row_count, -1), new_im.reshape(row_count, -1)])
    return (mixed_rows, updated)


def grid_sizes(ep_count, tp_count):
    inner = max(k for k in range(1, ep_count + 1) if ep_count % k == 0 and k * k <= ep_count)
    return {"z": ep_count // inner, "x": inner, "y": tp_count // 2, "c": 2}


def place_of(sizes):
    ep_place, tp_place = lax.axis_index("ep"), lax.axis_index("tp")
    return {
        "z": ep_place // sizes["x"],
        "x": ep_place % sizes["x"],
        "y": tp_place // 2,
        "c": tp_place % 2,
    }


def moved(sizes, place, offset):
    return {
        axis: (place[axis] + offset[axis]) % sizes[axis] if offset.get(axis) else place[axis]
        for axis in place
    }


def device_at(sizes, place):
    return {"ep": place["z"] * sizes["x"] + place["x"], "tp": place["y"] * 2 + place["c"]}


def block_at(sizes, axes, place):
    index = 0
    for axis in axes:
        index = index * sizes[axis] + place[axis]
    return index


def rank_at(sizes, axes, offset):
    return block_at(sizes, axes, {axis: offset.get(axis, 0) for axis in axes})


def greet(sizes, axes, place):
    barrier = pltpu.get_barrier_semaphore()
    count = 0
    for axis in axes:
        for step in range(1, sizes[axis]):
            pl.semaphore_signal(
                barrier,
                inc=1,
                device_id=device_at(sizes, moved(sizes, place, {axis: step})),
                device_id_type=pl.DeviceIdType.MESH,
            )
            count += 1
    pl.semaphore_wait(barrier, count)


def offsets_over(sizes, axes):
    for steps in itertools.product(*[range(sizes[axis]) for axis in axes]):
        yield dict(zip(axes, steps))


def gather_kernel(sizes, axes, parts, in_ref, out_ref, send_sem, recv_sem, own_sem):
    place = place_of(sizes)
    total = 1
    for axis in axes:
        total *= sizes[axis]
    own = block_at(sizes, axes, place)
    own_copy = pltpu.make_async_copy(in_ref, out_ref.at[own], own_sem)
    own_copy.start()
    greet(sizes, axes, place)

    def columns(ref, part):
        return ref.at[:, pl.ds(parts[part][1], parts[part][2])]

    def copy_of(source, part, block, rank, peer):
        return pltpu.make_async_remote_copy(
            src_ref=columns(source, part),
            dst_ref=columns(out_ref.at[block], part),
            send_sem=send_sem,
            recv_sem=recv_sem.at[part, rank],
            device_id=device_at(sizes, peer),
            device_id_type=pl.DeviceIdType.MESH,
        )

    for stage in range(len(axes) + 1):
        lists = []
        for part, (order, _, _) in enumerate(parts):
            todo = []
            if stage == 0:
                todo.append({})
            else:
                for offset in offsets_over(sizes, order[:stage]):
                    if offset[order[stage - 1]]:
                        todo.append(offset)
                todo.sort(key=lambda o: [bool(o[a]) for a in order[:stage]])
            lists.append([(part, order, offset) for offset in todo])
        for items in itertools.zip_longest(*lists):
            for item in items:
                if item is None:
                    continue
                part, order, offset = item
                block = block_at(sizes, axes, moved(sizes, place, offset))
                source = in_ref if stage == 0 else out_ref.at[block]
                if stage:
                    copy_of(
                        source, part, block, rank_at(sizes, axes, offset), moved(sizes, place, {order[0]: 1})
                    ).wait_recv()
                for axis in order[stage:]:
                    for step in range(1, sizes[axis]):
                        seen = dict(offset)
                        seen[axis] = sizes[axis] - step
                        copy_of(
                            source,
                            part,
                            block,
                            rank_at(sizes, axes, seen),
                            moved(sizes, place, {axis: step}),
                        ).start()
    own_copy.wait()
    sent = out_ref.at[pl.ds(0, total - 1)]
    pltpu.make_async_copy(sent, sent, send_sem).wait()


def gather_blocks(sizes, axes, parts, block, collective_id):
    total = 1
    for axis in axes:
        total *= sizes[axis]
    vmem = pl.BlockSpec(memory_space=pltpu.VMEM)
    return pl.pallas_call(
        functools.partial(gather_kernel, sizes, axes, parts),
        out_shape=jax.ShapeDtypeStruct((total,) + block.shape, block.dtype),
        in_specs=[vmem],
        out_specs=vmem,
        scratch_shapes=[
            pltpu.SemaphoreType.DMA,
            pltpu.SemaphoreType.DMA((len(parts), total)),
            pltpu.SemaphoreType.DMA,
        ],
        compiler_params=pltpu.CompilerParams(collective_id=collective_id, has_side_effects=True),
    )(block)


def scatter_kernel(
    sizes, axes, parts, in_ref, base_ref, out_ref, recv_ref, sum_ref, send_sem, recv_sem
):
    place = place_of(sizes)
    total = in_ref.shape[0]
    half = parts[0][2]
    greet(sizes, axes, place)
    slot_at = [0] * len(parts)
    waiting = []

    def flush():
        for copy in waiting:
            copy.start()
        waiting.clear()

    def columns(ref, part):
        return ref.at[:, pl.ds(parts[part][1], half)]

    def held(part, order, stage, offset):
        if stage == 0:
            return columns(in_ref.at[block_at(sizes, axes, moved(sizes, place, offset))], part)
        return sum_ref.at[part, rank_at(sizes, order[1:], offset)]

    def slot_of(part, order, stage, step, offset):
        rest = order[stage + 1 :]
        count = 1
        for axis in rest:
            count *= sizes[axis]
        return slot_at[part] + (step - 1) * count + rank_at(sizes, rest, offset)

    def send_of(part, order, stage, offset):
        axis = order[stage]
        slot = slot_of(part, order, stage, offset[axis], offset)
        return pltpu.make_async_remote_copy(
            src_ref=held(part, order, stage, offset),
            dst_ref=recv_ref.at[part, slot],
            send_sem=send_sem,
            recv_sem=recv_sem.at[part, slot],
            device_id=device_at(sizes, moved(sizes, place, {axis: offset[axis]})),
            device_id_type=pl.DeviceIdType.MESH,
        )

    def sorted_offsets(order, stage):
        todo = list(offsets_over(sizes, order[stage:]))
        todo.sort(key=lambda o: [not o[axis] for axis in order[stage:]])
        return todo

    def interleave(lists):
        for items in itertools.zip_longest(*lists):
            for item in items:
                if item is not None:
                    yield item

    firsts = []
    for part, (order, _, _) in enumerate(parts):
        todo = [o for o in sorted_offsets(order, 0) if o[order[0]]]
        firsts.append([(part, order, o) for o in todo])
    for part, order, offset in interleave(firsts):
        send_of(part, order, 0, offset).start()
    depth = len(axes)
    for stage in range(depth):
        lists = []
        for part, (order, _, _) in enumerate(parts):
            lists.append([(part, order, o) for o in sorted_offsets(order, stage + 1)])
        begun = list(slot_at)
        for part, order, offset in interleave(lists):
            before = dict(offset)
            before[order[stage]] = 0
            value = held(part, order, stage, before)[...].astype(jnp.float32)
            for step in range(1, sizes[order[stage]]):
                slot = slot_of(part, order, stage, step, offset)
                arrived = recv_ref.at[part, slot]
                pltpu.make_async_copy(arrived, arrived, recv_sem.at[part, slot]).wait()
                value = value + arrived[...].astype(jnp.float32)
            if stage == depth - 1:
                where = pl.ds(parts[part][1], half)
                out_ref[:, where] = (base_ref[:, where] + value).astype(out_ref.dtype)
                continue
            sum_ref[part, rank_at(sizes, order[1:], offset)] = value.astype(sum_ref.dtype)
            flush()
            if offset[order[stage + 1]]:
                count = 1
                for axis in order[stage + 1 :]:
                    count *= sizes[axis]
                slot_at[part] = begun[part] + (sizes[order[stage]] - 1) * count
                waiting.append(send_of(part, order, stage + 1, offset))
                slot_at[part] = begun[part]
        flush()
        for part, (order, _, _) in enumerate(parts):
            count = 1
            for axis in order[stage + 1 :]:
                count *= sizes[axis]
            slot_at[part] = begun[part] + (sizes[order[stage]] - 1) * count
    for part in range(len(parts)):
        sent = recv_ref.at[part]
        pltpu.make_async_copy(sent, sent, send_sem).wait()


def scatter_blocks(sizes, axes, parts, blocks, base, collective_id):
    total, rows, width = blocks.shape
    half = parts[0][2]
    vmem = pl.BlockSpec(memory_space=pltpu.VMEM)
    return pl.pallas_call(
        functools.partial(scatter_kernel, sizes, axes, parts),
        out_shape=jax.ShapeDtypeStruct((rows, width), jnp.bfloat16),
        in_specs=[vmem, vmem],
        out_specs=vmem,
        scratch_shapes=[
            pltpu.VMEM((len(parts), total - 1, rows, half), jnp.bfloat16),
            pltpu.VMEM((len(parts), total // 2, rows, half), jnp.bfloat16),
            pltpu.SemaphoreType.DMA,
            pltpu.SemaphoreType.DMA((len(parts), total)),
        ],
        compiler_params=pltpu.CompilerParams(
            collective_id=collective_id, has_side_effects=True, vmem_limit_bytes=48 * 2**20
        ),
    )(blocks, base)


def three_terms(values):
    first = values.astype(jnp.bfloat16)
    rest = values - first.astype(jnp.float32)
    second = rest.astype(jnp.bfloat16)
    third = (rest - second.astype(jnp.float32)).astype(jnp.bfloat16)
    return [first, second, third]


def per_device(
    residual,
    in_gain,
    in_weight,
    state,
    decay_rate,
    frequency,
    log_step,
    in_coef,
    out_coef,
    skip_gain,
    out_weight,
    mid_gain,
    gate_vector,
    routes,
    route_weight,
    expert_gate,
    expert_up,
    expert_down,
    shared_gate,
    shared_up,
    shared_down,
):
    tp_count = lax.axis_size("tp")
    ep_count = lax.axis_size("ep")
    tp_place = lax.axis_index("tp")
    ep_place = lax.axis_index("ep")
    seq_rows, feat_part = residual.shape
    width = feat_part * tp_count
    per_dev = seq_rows // tp_count
    experts = ep_count * tp_count
    top_count = routes.shape[1]
    capacity = max(2, 2 * seq_rows * top_count // experts)
    sizes = grid_sizes(ep_count, tp_count)

    def gather_features(values, collective_id):
        parts = [("yc", 0, values.shape[1])]
        blocks = gather_blocks(sizes, "yc", parts, values, collective_id)
        return jnp.swapaxes(blocks, 0, 1).reshape(seq_rows, -1)

    full_resid = gather_features(residual, 0).astype(jnp.float32)
    normed = layer_norm(full_resid, in_gain).astype(jnp.bfloat16)
    mixed_part, new_state = mixer_step(
        normed, in_weight, state, decay_rate, frequency, log_step, in_coef, out_coef, skip_gain
    )
    mixed_rows = gather_features(mixed_part, 1)

    own_rows = lambda values: lax.dynamic_slice_in_dim(values, tp_place * per_dev, per_dev, 0)
    own_after = own_rows(full_resid) + jnp.dot(
        own_rows(mixed_rows), out_weight, preferred_element_type=jnp.float32
    )
    own_mid = layer_norm(own_after, mid_gain).astype(jnp.bfloat16)
    weights = route_weight / jnp.sum(route_weight, axis=-1, keepdims=True) * routed_scale
    tail = [own_rows(routes).astype(jnp.bfloat16)] + three_terms(own_rows(weights))
    tail.append(jnp.zeros((per_dev, lanes - 4 * top_count), jnp.bfloat16))
    sent = jnp.concatenate([own_mid] + tail, axis=1)
    half = width // 2
    parts = [("zxyc", 0, half), ("zyxc", half, sent.shape[1] - half)]
    got = gather_blocks(sizes, "zxyc", parts, sent, 2).reshape(-1, sent.shape[1])

    rows = got[:, :width].reshape(ep_count, seq_rows, width)
    extra = got[:, width:].astype(jnp.float32)
    ids = extra[:, :top_count]
    parts = [extra[:, top_count * k : top_count * (k + 1)] for k in (1, 2, 3)]
    weight_of = (parts[0] + parts[1]) + parts[2]
    mine = (ep_place * tp_count + tp_place).astype(jnp.float32)
    hits = ids == mine
    hit = jnp.any(hits, axis=1).reshape(ep_count, seq_rows)
    hit_weight = jnp.sum(jnp.where(hits, weight_of, 0.0), axis=1).reshape(ep_count, seq_rows)
    places = jnp.arange(seq_rows)
    earlier = (places[:, None] < places[None, :]).astype(jnp.bfloat16)
    rank = jnp.dot(hit.astype(jnp.bfloat16), earlier, preferred_element_type=jnp.float32)
    chosen = hit[:, None, :] & (
        rank[:, None, :] == jnp.arange(capacity, dtype=jnp.float32)[None, :, None]
    )
    onehot = chosen.astype(jnp.bfloat16)
    slot_weight = jnp.sum(jnp.where(chosen, hit_weight[:, None, :], 0.0), axis=2)
    picked = jnp.einsum("gjr,grd->gjd", onehot, rows, preferred_element_type=jnp.float32)
    picked = picked.astype(jnp.bfloat16).reshape(ep_count * capacity, width)

    def two_layers(values, gate_weight, up_weight, down_weight):
        gate_part = jnp.dot(values, gate_weight, preferred_element_type=jnp.float32)
        up_part = jnp.dot(values, up_weight, preferred_element_type=jnp.float32)
        hidden = (jax.nn.silu(gate_part) * up_part).astype(jnp.bfloat16)
        return jnp.dot(hidden, down_weight, preferred_element_type=jnp.float32)

    result = two_layers(picked, expert_gate[0], expert_up[0], expert_down[0])
    result = (result * slot_weight.reshape(-1)[:, None]).astype(jnp.bfloat16)
    spread = jnp.einsum(
        "gjr,gjd->grd",
        onehot,
        result.reshape(ep_count, capacity, width),
        preferred_element_type=jnp.float32,
    )
    piece = lax.dynamic_slice_in_dim(rows, tp_place * per_dev, per_dev, 1).reshape(-1, width)
    gate_value = jax.nn.sigmoid(jnp.dot(piece, gate_vector, preferred_element_type=jnp.float32))
    shared = two_layers(piece, shared_gate, shared_up, shared_down) * gate_value[:, None]
    is_own = (jnp.arange(tp_count) == tp_place)[None, :, None, None]
    total = spread.reshape(ep_count, tp_count, per_dev, width) + jnp.where(
        is_own, shared.reshape(ep_count, 1, per_dev, width), 0.0
    )
    total = total.astype(jnp.bfloat16).reshape(-1, per_dev, width)
    parts = [("cyxz", 0, half), ("cxyz", half, half)]
    layer_out = scatter_blocks(sizes, "zxyc", parts, total, own_after, 3)
    return (layer_out, new_state)


def solution(mesh):
    return jax.shard_map(
        per_device,
        mesh=mesh,
        in_specs=(
            P("ep", "tp"),
            P(),
            P(None, "tp"),
            P(None, "ep", "tp"),
            P("tp", None),
            P("tp", None),
            P("tp"),
            P(None, "tp", None, None),
            P(None, "tp", None, None),
            P("tp"),
            P(),
            P(),
            P(),
            P("ep", None),
            P("ep", None),
            P(("ep", "tp"), None, None),
            P(("ep", "tp"), None, None),
            P(("ep", "tp"), None, None),
            P(None, "ep"),
            P(None, "ep"),
            P("ep", None),
        ),
        out_specs=(P(("ep", "tp"), None), P(None, "ep", "tp")),
        check_vma=False,
    )
```

time: 210 us -> 152 us (0.72)
  Pallas kernels: 0 us -> 83.5 us
  waiting for transfers between devices: 79.4 us -> 0 us
  blocking collectives: 29.4 us -> 0 us
  starting transfers between devices: 17.5 us -> 0 us
  between operations: 14.3 us -> 0.97 us
  other arithmetic: 17 us -> 14.1 us
    pallas_call x0 -> x4, Pallas kernels: none -> 83.5 us  [the longest x3 50.4 us: gather_blocks(): pl.pallas_call(functools.partial(gather_kernel, sizes, axes, parts), out_...]
    all_to_all x4 -> x0, waiting for transfers between devices: 69.2 us -> none  [the longest x1 26.4 us: per_device(): lax.all_to_all(outgoing, 'ep', split_axis=0, concat_axis=0, tiled=True)]
    all_gather x3 -> x0, blocking collectives: 23.4 us -> none  [the longest x1 10.3 us: per_device(): lax.all_gather(residual, 'tp', axis=1, tiled=True)]
    all_to_all x4 -> x0, starting transfers between devices: 17.3 us -> none  [the longest x1 5.81 us: per_device(): lax.all_to_all(outgoing, 'ep', split_axis=0, concat_axis=0, tiled=True)]
    reduce_scatter x1 -> x0, waiting for transfers between devices: 10.2 us -> none  [per_device(): lax.psum_scatter(routed_part.astype(jnp.bfloat16), 'tp', scatter_dimensio...]
    reduce_sum x5 -> x3, other arithmetic: 8.99 us -> 2.11 us  [the longest x1 1.35 us: layer_norm(): row_mean = jnp.mean(values, axis=-1, keepdims=True)]
    psum x1 -> x0, blocking collectives: 5.97 us -> none  [per_device(): lax.psum((jnp.sum(own_values, axis=1), jnp.sum(own_values * own_values, a...]
    gather x2 -> x0, local copies, waits for them, and re-layouts: 5.66 us -> none  [the longest x1 3.33 us: per_device(): picked = flat_back[jnp.where(is_mine, slot_place, 0)].astype(jnp.float32)]
  transfers between devices with their start and end apart: 5 -> 0, of which waited for: 5 -> 0; matrix products, arithmetic and copies ran while one was open for 17% -> 0% of each run, Pallas kernels for 0% -> 0%
where the time goes in v1:
time: 152 us; the launch traced here: 150 us
  Pallas kernels  83.5 us (55%)
  matrix products  29 us (19%)
  local copies, waits for them, and re-layouts  22.8 us (15%)
  other arithmetic  14.1 us (9%)
    pallas_call x3, Pallas kernels, gather_blocks(): pl.pallas_call(functools.partial(gather_kernel, sizes, axes, parts), out_...  50.4 us
    pallas_call x1, Pallas kernels, scatter_blocks(): pl.pallas_call(functools.partial(scatter_kernel, sizes, axes, parts), out...  33 us
    dot_general x2, matrix products, two_layers(): return jnp.dot(hidden, down_weight, preferred_element_type=jnp.float32)  9.42 us
    slice x1, local copies, waits for them, and re-layouts, per_device(): rows = got[:, :width].reshape(ep_count, seq_rows, width)  4.76 us
    dot_general x2, matrix products, two_layers(): gate_part = jnp.dot(values, gate_weight, preferred_element_type=jnp.float32)  4.61 us
    slice x2, local copies, waits for them, and re-layouts, mixer_step(): old_re = state[0].reshape(row_count, group_count, state_count)  4.33 us
    dot_general x1, matrix products, per_device(): jnp.dot(own_rows(mixed_rows), out_weight, preferred_element_type=jnp.floa...  3.36 us
    convert_element_type x1, other arithmetic, per_device(): total = total.astype(jnp.bfloat16).reshape(-1, per_dev, width)  3.18 us

profile of v1, /device:TPU:0, one launch (start us, length us, event | category | flops | bytes accessed | tf_op | source)
XLA Modules:
  0.0 150.3 jit_solution(4238231668924490593)
XLA Ops:
  0.7 0.8 exp.16
  1.5 0.6 broadcast_in_dim.78
  2.1 0.7 reduce_sum.67
  2.8 0.7 divide_multiply_fusion
  3.5 0.8 constant_dynamic-slice_fusion.1
  4.3 0.7 reshape.105
  5.2 0.6 subtract_convert_fusion
  5.8 0.8 add_divide_fusion
  6.6 10.1 %shard_map.212 = bf16[4,128,512]{2,1,0:T(8,128)(2,1)} custom-call(bf16[128,512]{1,0:T(8,128)(2,1)} %in_ref.1), custom_call_target="tpu_custom_call" | custom-call | tf_op jit(solution)/shard_map/pallas_call | solution.py:184
  16.7 1.3 convert_reduce_fusion
  18.1 1.2 convert_bitcast_fusion
  19.4 0.3 convolution_convert_fusion.1
  19.7 0.1 copy.50
  19.8 2.3 %fusion.79 = (f32[1,128,1024]{2,1,0:T(8,128)}, f32[1,128,1024]{2,1,0:T(8,128)}) fusion(f32[2,128,1024]{2,1,0:T(8,128)} %param.24), kind=kLoop, calls=%fused_computation.116 | loop fusion | bytes 2097152 | tf_op jit(solution)/shard_map/slice | solution.py:47
  22.1 2.1 %copy.48 = f32[1,128,1024]{1,2,0:T(8,128)} copy(f32[1,128,1024]{2,1,0:T(8,128)} %get-tuple-element.8) | data formatting | bytes 1048576 | tf_op jit(solution)/shard_map/slice | solution.py:47
  24.2 2.0 %copy.49 = f32[1,128,1024]{1,2,0:T(8,128)} copy(f32[1,128,1024]{2,1,0:T(8,128)} %get-tuple-element.9) | data formatting | bytes 1048576 | tf_op jit(solution)/shard_map/slice | solution.py:48
  26.2 2.2 %fusion.11 = f32[128,16,64]{0,2,1:T(8,128)S(1)} fusion(bf16[128,16,16]{0,2,1:T(8,128)(2,1)S(1)} %bitcast.118, f32[128,16,64]{0,2,1:T(8,128)} %bitcast.103, f32[128,16,64]{0,2,1:T(8,128)} %bitcast.105, f32[16,64]{1,0:T(8,128)S(1)} %get-tuple-element.13, f32[16,64]{1,0:T(8,128)S(1)} %get-tuple-element.11, f32[2,16,64,16]{2,3,1,0:T(8,128)} %param.28, ...), kind=kOutput, calls=%fused_computation.19 | convolution fusion | flops 25739264 | bytes 1785856 | tf_op jit(solution)/shard_map/tgh,gph->tgp/dot_general | solution.py:46
  28.5 1.9 %fusion.12 = f32[128,16,64]{0,2,1:T(8,128)S(1)} fusion(bf16[128,16,16]{0,2,1:T(8,128)(2,1)S(1)} %bitcast.119, f32[128,16,64]{0,2,1:T(8,128)S(1)} %bitcast.106, f32[128,16,64]{0,2,1:T(8,128)S(1)} %bitcast.104, f32[16,64]{1,0:T(8,128)S(1)} %get-tuple-element.13, f32[16,64]{1,0:T(8,128)S(1)} %get-tuple-element.11, f32[2,16,64,16]{2,3,1,0:T(8,128)} %param.28, ...), kind=kOutput, calls=%fused_computation.21 | convolution fusion | flops 25739264 | bytes 1785856 | tf_op jit(solution)/shard_map/tgh,gph->tgp/dot_general | solution.py:45
  30.4 0.8 copy-done.3
  31.2 0.6 fusion.47
  31.8 0.6 convolution_subtract_fusion
  32.4 1.4 fusion.45.in_ref
  33.8 6.9 %shard_map.213 = bf16[4,128,256]{2,1,0:T(8,128)(2,1)} custom-call(bf16[128,256]{1,0:T(8,128)(2,1)} %fusion.45.in_ref), custom_call_target="tpu_custom_call" | custom-call | tf_op jit(solution)/shard_map/pallas_call | solution.py:184
  40.7 1.8 %copy.52 = bf16[128,4,256]{0,2,1:T(8,128)(2,1)} copy(bf16[128,4,256]{2,0,1:T(8,128)(2,1)} %bitcast.117) | data formatting | bytes 524288 | tf_op jit(solution)/shard_map/transpose | solution.py:363
  42.5 3.4 %fusion.77 = (f32[32]{0:T(128)S(1)}, f32[32]{0:T(128)S(1)}, f32[32,2048]{1,0:T(8,128)S(1)}) fusion(bf16[1024,2048]{1,0:T(8,128)(2,1)} %param.31, bf16[128,1024]{0,1:T(8,128)(2,1)} %bitcast.116, s32[]{:T(128)S(6)} %select_n.20, f32[128,2048]{1,0:T(8,128)S(1)} %bitcast.102), kind=kOutput, calls=%fused_computation.114 | convolution fusion | flops 134479808 | bytes 4982016 | tf_op jit(solution)/shard_map/dot_general | solution.py:373
  46.1 0.8 concatenate.3.in_ref
  46.8 1.2 copy.56
  48.1 1.0 copy.55
  49.1 2.1 %pad_maximum_fusion = f32[2,128,1024]{2,1,0:T(8,128)} fusion(f32[1,128,1024]{2,1,0:T(8,128)S(1)} %copy.56, f32[1,128,1024]{2,1,0:T(8,128)} %copy.55), kind=kLoop, calls=%fused_computation.27 | loop fusion | flops 262144 | bytes 2097152 | tf_op jit(solution)/shard_map/stack | solution.py:56
  51.2 33.4 %shard_map.214 = bf16[32,32,2176]{2,1,0:T(8,128)(2,1)} custom-call(bf16[32,2176]{1,0:T(8,128)(2,1)} %concatenate.3.in_ref), custom_call_target="tpu_custom_call" | custom-call | tf_op jit(solution)/shard_map/pallas_call | solution.py:184
  84.6 1.0 slice_convert_fusion
  85.6 4.8 %slice.52 = bf16[1024,2048]{1,0:T(8,128)(2,1)} slice(bf16[1024,2176]{1,0:T(8,128)(2,1)} %bitcast.100), slice={[0:1024], [0:2048]} | slice | bytes 8388608 | tf_op jit(solution)/shard_map/slice | solution.py:385
  90.4 0.2 fusion.78
  90.6 0.6 fusion.21
  91.2 0.1 fusion.71
  91.4 0.1 select_reduce_fusion
  91.6 1.3 constant_dynamic-slice_fusion.2
  92.9 3.0 %convolution_convert_fusion = bf16[8,32,2048]{2,1,0:T(8,128)(2,1)S(1)} fusion(bf16[8,128,2048]{2,1,0:T(8,128)(2,1)} %bitcast.98, f32[8,128]{1,0:T(8,128)S(1)} %fusion.71, pred[8,128]{1,0:T(8,128)(4,1)S(1)} %bitcast.122), kind=kOutput, calls=%fused_computation.6 | convolution fusion | flops 134807552 | bytes 5248000 | tf_op jit(solution)/shard_map/gjr,grd->gjd/dot_general | solution.py:402
  95.9 0.4 fusion.81
  96.3 0.6 copy-done.6
  96.9 1.5 %fusion.6 = f32[256,512]{1,0:T(8,128)} fusion(bf16[256,2048]{1,0:T(8,128)(2,1)S(1)} %bitcast.114, bf16[1,2048,512]{2,1,0:T(8,128)(2,1)S(1)} %copy-done.15), kind=kOutput, calls=%fused_computation.11 | convolution fusion | flops 536870912 | bytes 3670016 | tf_op jit(solution)/shard_map/dot_general | solution.py:406
  98.4 4.3 %fusion.2 = bf16[256,2048]{1,0:T(8,128)(2,1)} fusion(bf16[1,512,2048]{2,1,0:T(8,128)(2,1)S(1)} %copy-done, f32[256]{0:T(256)S(1)} %mul.280, bf16[256,2048]{1,0:T(8,128)(2,1)} %bitcast.115, bf16[1,2048,512]{2,1,0:T(8,128)(2,1)} %param.37, f32[256,512]{1,0:T(8,128)} %fusion.6), kind=kOutput, calls=%fused_computation.5 | convolution fusion | flops 1075576832 | bytes 6816768 | tf_op jit(solution)/shard_map/dot_general | solution.py:409
  102.7 3.1 %fusion.80 = f32[256,512]{1,0:T(8,128)} fusion(bf16[256,2048]{1,0:T(8,128)(2,1)S(1)} %bitcast.110, bf16[2048,512]{1,0:T(8,128)(2,1)} %param.39), kind=kOutput, calls=%fused_computation.117 | convolution fusion | flops 536870912 | bytes 3670016 | tf_op jit(solution)/shard_map/dot_general | solution.py:406
  105.8 5.1 %convolution_multiply_fusion = f32[256,2048]{1,0:T(8,128)} fusion(bf16[512,2048]{1,0:T(8,128)(2,1)} %param.41, bf16[256,2048]{1,0:T(8,128)(2,1)S(1)} %bitcast.111, bf16[2048,512]{1,0:T(8,128)(2,1)} %param.40, f32[256]{0:T(256)S(1)} %add_divide_fusion.1, f32[256,512]{1,0:T(8,128)} %fusion.80), kind=kOutput, calls=%fused_computation.3 | convolution fusion | flops 1075052544 | bytes 7865344 | tf_op jit(solution)/shard_map/dot_general | solution.py:409
  110.9 2.5 %fusion.56 = f32[8,128,2048]{2,1,0:T(8,128)S(1)} fusion(bf16[8,32,2048]{2,1,0:T(8,128)(2,1)} %bitcast.113, f32[8,128]{1,0:T(8,128)S(1)} %fusion.71, pred[8,128]{1,0:T(8,128)(4,1)S(1)} %bitcast.123), kind=kOutput, calls=%fused_computation.76 | convolution fusion | flops 134283264 | bytes 9442304 | tf_op jit(solution)/shard_map/gjr,gjd->grd/dot_general | solution.py:413
  113.5 3.2 %fusion.1.in_ref = bf16[32,32,2048]{2,1,0:T(8,128)(2,1)S(1)} fusion(f32[32,32,2048]{2,1,0:T(8,128)S(1)} %bitcast.96, f32[8,32,2048]{2,1,0:T(8,128)} %bitcast.112, pred[32]{0:T(512)(128)(4,1)S(1)} %copy-done.14), kind=kLoop, calls=%fused_computation.2 | loop fusion | flops 6291456 | bytes 14680096 | tf_op jit(solution)/shard_map/convert_element_type | solution.py:426
  116.6 33.0 %shard_map.215 = bf16[32,2048]{1,0:T(8,128)(2,1)S(1)} custom-call(bf16[32,32,2048]{2,1,0:T(8,128)(2,1)S(1)} %fusion.1.in_ref, f32[32,2048]{1,0:T(8,128)S(1)} %get-tuple-element.21.base_ref), custom_call_target="tpu_custom_call" | custom-call | tf_op jit(solution)/shard_map/pallas_call | solution.py:300
  149.7 0.7 copy.61
  (44 shorter events, 0.7 us)
Async XLA Ops:
  0.6 97.8 %copy-start = (bf16[1,512,2048]{2,1,0:T(8,128)(2,1)S(1)}, bf16[1,512,2048]{2,1,0:T(8,128)(2,1)}, u32[]{:S(2)}) copy-start(bf16[1,512,2048]{2,1,0:T(8,128)(2,1)} %param.38) | copy-start | bytes 6291460
  16.7 2.7 %copy-start.7 = (bf16[2048,256]{1,0:T(8,128)(2,1)S(1)}, bf16[2048,256]{1,0:T(8,128)(2,1)}, u32[]{:S(2)}) copy-start(bf16[2048,256]{1,0:T(8,128)(2,1)} %param.23) | copy-start | bytes 3145732
  16.7 2.7 %copy-start.12 = (f32[2048]{0:T(1024)S(1)}, f32[2048]{0:T(1024)}, u32[]{:S(2)}) copy-start(f32[2048]{0:T(1024)} %param.22) | copy-start | bytes 24580
  26.2 2.2 %copy-start.1 = (f32[1,128,1024]{1,2,0:T(8,128)S(1)}, f32[1,128,1024]{1,2,0:T(8,128)}, u32[]{:S(2)}) copy-start(f32[1,128,1024]{1,2,0:T(8,128)} %copy.48) | copy-start | bytes 1572868
  26.2 2.2 %copy-start.2 = (f32[1,128,1024]{1,2,0:T(8,128)S(1)}, f32[1,128,1024]{1,2,0:T(8,128)}, u32[]{:S(2)}) copy-start(f32[1,128,1024]{1,2,0:T(8,128)} %copy.49) | copy-start | bytes 1572868
  26.2 5.0 %copy-start.8 = (f32[2,16,16,64]{3,2,1,0:T(8,128)S(1)}, f32[2,16,16,64]{3,2,1,0:T(8,128)}, u32[]{:S(2)}) copy-start(f32[2,16,16,64]{3,2,1,0:T(8,128)} %param.29) | copy-start | bytes 393220
  28.4 3.3 %copy-start.5 = (f32[128,16,64]{0,2,1:T(8,128)}, f32[128,16,64]{0,2,1:T(8,128)S(1)}, u32[]{:S(2)}) copy-start(f32[128,16,64]{0,2,1:T(8,128)S(1)} %fusion.11) | copy-start | bytes 1572868
  30.4 0.8 copy-start.3
  42.5 3.4 %copy-start.13 = (f32[2048]{0:T(1024)S(1)}, f32[2048]{0:T(1024)}, u32[]{:S(2)}) copy-start(f32[2048]{0:T(1024)} %param.32) | copy-start | bytes 24580
  42.5 3.5 %copy-start.9 = (bf16[32,4]{1,0:T(8,128)(2,1)S(1)}, bf16[32,4]{1,0:T(8,128)(2,1)}, u32[]{:S(2)}) copy-start(bf16[32,4]{1,0:T(8,128)(2,1)} %get-tuple-element.14) | copy-start | bytes 772
  42.5 3.5 %copy-start.10 = (bf16[32,4]{1,0:T(8,128)(2,1)S(1)}, bf16[32,4]{1,0:T(8,128)(2,1)}, u32[]{:S(2)}) copy-start(bf16[32,4]{1,0:T(8,128)(2,1)} %get-tuple-element.15) | copy-start | bytes 772
  42.5 3.5 %copy-start.11 = (bf16[32,4]{1,0:T(8,128)(2,1)S(1)}, bf16[32,4]{1,0:T(8,128)(2,1)}, u32[]{:S(2)}) copy-start(bf16[32,4]{1,0:T(8,128)(2,1)} %get-tuple-element.16) | copy-start | bytes 772
  45.9 2.2 %copy-start.4 = (f32[128,16,64]{0,2,1:T(8,128)S(1)}, f32[128,16,64]{0,2,1:T(8,128)}, u32[]{:S(2)}) copy-start(f32[128,16,64]{0,2,1:T(8,128)} %copy-done.3) | copy-start | bytes 1572868
  92.9 4.0 %copy-start.15 = (bf16[1,2048,512]{2,1,0:T(8,128)(2,1)S(1)}, bf16[1,2048,512]{2,1,0:T(8,128)(2,1)}, u32[]{:S(2)}) copy-start(bf16[1,2048,512]{2,1,0:T(8,128)(2,1)} %param.36) | copy-start | bytes 6291460
  95.9 1.0 copy-start.6
  110.9 2.5 %copy-start.14 = (pred[32]{0:T(512)(128)(4,1)S(1)}, pred[32]{0:T(512)(128)(4,1)}, u32[]{:S(2)}) copy-start(pred[32]{0:T(512)(128)(4,1)} %broadcast_in_dim.78) | copy-start | bytes 100

commit v2 on v1

--- a/solution.py
+++ b/solution.py
@@ -33,28 +33,75 @@
     return (keep_re, keep_im, push_re, push_im)
 
 
+def mixer_kernel(
+    normed_ref,
+    in_weight_ref,
+    state_ref,
+    keep_ref,
+    push_ref,
+    pull_ref,
+    skip_ref,
+    mixed_ref,
+    new_ref,
+):
+    highest = lax.Precision.HIGHEST
+    drive = jnp.dot(normed_ref[...], in_weight_ref[...], preferred_element_type=jnp.float32)
+    drive = drive.astype(jnp.bfloat16).astype(jnp.float32)
+
+    def product(left, right):
+        return jnp.dot(left, right, precision=highest, preferred_element_type=jnp.float32)
+
+    shape = (drive.shape[1], state_ref.shape[2])
+    group_ch = push_ref.shape[1]
+    copies = shape[0] // group_ch
+    row_group = lax.broadcasted_iota(jnp.int32, shape, 0) // group_ch
+    entry_group = lax.broadcasted_iota(jnp.int32, shape, 1) // (shape[1] // copies)
+    same = row_group == entry_group
+
+    def dense(values):
+        return jnp.where(same, jnp.concatenate([values] * copies, axis=0), 0.0)
+
+    def product_t(left, right):
+        return lax.dot_general(
+            left,
+            right,
+            (((1,), (1,)), ((), ())),
+            precision=highest,
+            preferred_element_type=jnp.float32,
+        )
+
+    keep_re, keep_im = keep_ref[0:1, :], keep_ref[1:2, :]
+    old_re, old_im = state_ref[0], state_ref[1]
+    new_re = keep_re * old_re - keep_im * old_im + product(drive, dense(push_ref[0]))
+    new_im = keep_re * old_im + keep_im * old_re + product(drive, dense(push_ref[1]))
+    new_ref[0] = new_re
+    new_ref[1] = new_im
+    read_out = product_t(new_re, dense(pull_ref[0])) - product_t(new_im, dense(pull_ref[1]))
+    read_out = read_out + skip_ref[...] * drive
+    mixed_ref[...] = jax.nn.gelu(read_out, approximate=True).astype(mixed_ref.dtype)
+
+
 def mixer_step(
     normed, in_weight, state, decay_rate, frequency, log_step, in_coef, out_coef, skip_gain
 ):
-    row_count = normed.shape[0]
-    group_count, state_count = decay_rate.shape
+    rows = normed.shape[0]
+    groups, entries = decay_rate.shape
+    channels = in_weight.shape[1]
     keep_re, keep_im, push_re, push_im = coefficients(decay_rate, frequency, log_step, in_coef)
-    drive = jnp.dot(normed, in_weight, preferred_element_type=jnp.float32).astype(jnp.bfloat16)
-    drive_f = drive.astype(jnp.float32).reshape(row_count, group_count, -1)
-    highest = lax.Precision.HIGHEST
-    input_re = jnp.einsum("tgh,gph->tgp", drive_f, push_re, precision=highest)
-    input_im = jnp.einsum("tgh,gph->tgp", drive_f, push_im, precision=highest)
-    old_re = state[0].reshape(row_count, group_count, state_count)
-    old_im = state[1].reshape(row_count, group_count, state_count)
-    new_re = keep_re * old_re - keep_im * old_im + input_re
-    new_im = keep_re * old_im + keep_im * old_re + input_im
-    read_out = jnp.einsum("ghp,tgp->tgh", out_coef[0], new_re, precision=highest) - jnp.einsum(
-        "ghp,tgp->tgh", out_coef[1], new_im, precision=highest
-    )
-    read_out = read_out.reshape(row_count, -1) + skip_gain * drive_f.reshape(row_count, -1)
-    mixed_rows = jax.nn.gelu(read_out, approximate=True).astype(jnp.bfloat16)
-    updated = jnp.stack([new_re.reshape(row_count, -1), new_im.reshape(row_count, -1)])
-    return (mixed_rows, updated)
+    keep = jnp.stack([keep_re.reshape(-1), keep_im.reshape(-1)])
+    push = jnp.stack([push_re, push_im]).transpose(0, 3, 1, 2).reshape(2, -1, groups * entries)
+    pull = out_coef.transpose(0, 2, 1, 3).reshape(2, -1, groups * entries)
+    vmem = pl.BlockSpec(memory_space=pltpu.VMEM)
+    return pl.pallas_call(
+        mixer_kernel,
+        out_shape=(
+            jax.ShapeDtypeStruct((rows, channels), jnp.bfloat16),
+            jax.ShapeDtypeStruct(state.shape, jnp.float32),
+        ),
+        in_specs=[vmem] * 7,
+        out_specs=(vmem, vmem),
+        compiler_params=pltpu.CompilerParams(vmem_limit_bytes=24 * 2**20),
+    )(normed, in_weight, state, keep, push, pull, skip_gain.reshape(1, -1))
 
 
 def grid_sizes(ep_count, tp_count):
@@ -114,76 +161,74 @@
         yield dict(zip(axes, steps))
 
 
-def gather_kernel(sizes, axes, parts, in_ref, out_ref, send_sem, recv_sem, own_sem):
+def gather_kernel(sizes, axes, parts, wide, in_ref, out_ref, send_sem, recv_sem, own_sem):
     place = place_of(sizes)
     total = 1
     for axis in axes:
         total *= sizes[axis]
     own = block_at(sizes, axes, place)
-    own_copy = pltpu.make_async_copy(in_ref, out_ref.at[own], own_sem)
+
+    def spot(block):
+        if wide:
+            cols = in_ref.shape[1]
+            return out_ref.at[:, pl.ds(pl.multiple_of(block * cols, lanes), cols)]
+        return out_ref.at[block]
+
+    own_copy = pltpu.make_async_copy(in_ref, spot(own), own_sem)
     own_copy.start()
     greet(sizes, axes, place)
 
     def columns(ref, part):
-        return ref.at[:, pl.ds(parts[part][1], parts[part][2])]
+        return ref if wide else ref.at[:, pl.ds(parts[part][1], parts[part][2])]
 
     def copy_of(source, part, block, rank, peer):
         return pltpu.make_async_remote_copy(
             src_ref=columns(source, part),
-            dst_ref=columns(out_ref.at[block], part),
+            dst_ref=columns(spot(block), part),
             send_sem=send_sem,
             recv_sem=recv_sem.at[part, rank],
             device_id=device_at(sizes, peer),
             device_id_type=pl.DeviceIdType.MESH,
         )
 
-    for stage in range(len(axes) + 1):
-        lists = []
-        for part, (order, _, _) in enumerate(parts):
-            todo = []
-            if stage == 0:
-                todo.append({})
-            else:
-                for offset in offsets_over(sizes, order[:stage]):
-                    if offset[order[stage - 1]]:
-                        todo.append(offset)
-                todo.sort(key=lambda o: [bool(o[a]) for a in order[:stage]])
-            lists.append([(part, order, offset) for offset in todo])
-        for items in itertools.zip_longest(*lists):
-            for item in items:
-                if item is None:
-                    continue
-                part, order, offset = item
-                block = block_at(sizes, axes, moved(sizes, place, offset))
-                source = in_ref if stage == 0 else out_ref.at[block]
-                if stage:
-                    copy_of(
-                        source, part, block, rank_at(sizes, axes, offset), moved(sizes, place, {order[0]: 1})
-                    ).wait_recv()
-                for axis in order[stage:]:
-                    for step in range(1, sizes[axis]):
-                        seen = dict(offset)
-                        seen[axis] = sizes[axis] - step
-                        copy_of(
-                            source,
-                            part,
-                            block,
-                            rank_at(sizes, axes, seen),
-                            moved(sizes, place, {axis: step}),
-                        ).start()
+    events = []
+    for part, (order, _, _) in enumerate(parts):
+        delays = {axis: 2.5 + k for k, axis in enumerate(order)}
+        for offset in offsets_over(sizes, order):
+            steps = {axis: (sizes[axis] - offset[axis]) % sizes[axis] for axis in order}
+            arrival = sum(delays[axis] * steps[axis] for axis in order)
+            events.append((arrival, part, offset))
+    events.sort(key=lambda event: event[:2])
+    for _, part, offset in events:
+        order = parts[part][0]
+        stage = max([k + 1 for k, axis in enumerate(order) if offset[axis]], default=0)
+        block = block_at(sizes, axes, moved(sizes, place, offset))
+        source = spot(block) if stage else in_ref
+        if stage:
+            rank = rank_at(sizes, axes, offset)
+            copy_of(source, part, block, rank, moved(sizes, place, {order[0]: 1})).wait_recv()
+        for axis in order[stage:]:
+            for step in range(1, sizes[axis]):
+                seen = dict(offset)
+                seen[axis] = sizes[axis] - step
+                peer = moved(sizes, place, {axis: step})
+                copy_of(source, part, block, rank_at(sizes, axes, seen), peer).start()
     own_copy.wait()
-    sent = out_ref.at[pl.ds(0, total - 1)]
+    most = total - 1
+    sent = out_ref.at[:, pl.ds(0, most * in_ref.shape[1])] if wide else out_ref.at[pl.ds(0, most)]
     pltpu.make_async_copy(sent, sent, send_sem).wait()
 
 
-def gather_blocks(sizes, axes, parts, block, collective_id):
+def gather_blocks(sizes, axes, parts, block, collective_id, wide=False):
     total = 1
     for axis in axes:
         total *= sizes[axis]
+    rows, cols = block.shape
+    shape = (rows, total * cols) if wide else (total, rows, cols)
     vmem = pl.BlockSpec(memory_space=pltpu.VMEM)
     return pl.pallas_call(
-        functools.partial(gather_kernel, sizes, axes, parts),
-        out_shape=jax.ShapeDtypeStruct((total,) + block.shape, block.dtype),
+        functools.partial(gather_kernel, sizes, axes, parts, wide),
+        out_shape=jax.ShapeDtypeStruct(shape, block.dtype),
         in_specs=[vmem],
         out_specs=vmem,
         scratch_shapes=[
@@ -191,7 +236,11 @@
             pltpu.SemaphoreType.DMA((len(parts), total)),
             pltpu.SemaphoreType.DMA,
         ],
-        compiler_params=pltpu.CompilerParams(collective_id=collective_id, has_side_effects=True),
+        compiler_params=pltpu.CompilerParams(
+            collective_id=collective_id,
+            has_side_effects=True,
+            vmem_limit_bytes=(total + 2) * rows * cols * 2 + 4 * 2**20,
+        ),
     )(block)
 
 
@@ -202,7 +251,6 @@
     total = in_ref.shape[0]
     half = parts[0][2]
     greet(sizes, axes, place)
-    slot_at = [0] * len(parts)
     waiting = []
 
     def flush():
@@ -219,11 +267,13 @@
         return sum_ref.at[part, rank_at(sizes, order[1:], offset)]
 
     def slot_of(part, order, stage, step, offset):
+        base, left = 0, total
+        for axis in order[:stage]:
+            left //= sizes[axis]
+            base += (sizes[axis] - 1) * left
         rest = order[stage + 1 :]
-        count = 1
-        for axis in rest:
-            count *= sizes[axis]
-        return slot_at[part] + (step - 1) * count + rank_at(sizes, rest, offset)
+        count = left // sizes[order[stage]]
+        return base + (step - 1) * count + rank_at(sizes, rest, offset)
 
     def send_of(part, order, stage, offset):
         axis = order[stage]
@@ -237,57 +287,51 @@
             device_id_type=pl.DeviceIdType.MESH,
         )
 
-    def sorted_offsets(order, stage):
-        todo = list(offsets_over(sizes, order[stage:]))
-        todo.sort(key=lambda o: [not o[axis] for axis in order[stage:]])
-        return todo
-
-    def interleave(lists):
-        for items in itertools.zip_longest(*lists):
-            for item in items:
-                if item is not None:
-                    yield item
+    far = sizes["z"] // 2
+
+    def urgency(offset):
+        return abs(offset["z"] - far) if offset["z"] else sizes["z"]
 
     firsts = []
+    depth = len(axes)
+    events = []
     for part, (order, _, _) in enumerate(parts):
-        todo = [o for o in sorted_offsets(order, 0) if o[order[0]]]
-        firsts.append([(part, order, o) for o in todo])
-    for part, order, offset in interleave(firsts):
-        send_of(part, order, 0, offset).start()
-    depth = len(axes)
-    for stage in range(depth):
-        lists = []
-        for part, (order, _, _) in enumerate(parts):
-            lists.append([(part, order, o) for o in sorted_offsets(order, stage + 1)])
-        begun = list(slot_at)
-        for part, order, offset in interleave(lists):
-            before = dict(offset)
-            before[order[stage]] = 0
-            value = held(part, order, stage, before)[...].astype(jnp.float32)
-            for step in range(1, sizes[order[stage]]):
-                slot = slot_of(part, order, stage, step, offset)
-                arrived = recv_ref.at[part, slot]
-                pltpu.make_async_copy(arrived, arrived, recv_sem.at[part, slot]).wait()
-                value = value + arrived[...].astype(jnp.float32)
+        for offset in offsets_over(sizes, order):
+            if offset[order[0]]:
+                key = (urgency(offset), [not offset[axis] for axis in order])
+                firsts.append((key, part, offset))
+        for stage in range(depth):
+            for offset in offsets_over(sizes, order[stage + 1 :]):
+                z_step = offset.get("z", 0)
+                when = 3.0 * urgency({"z": z_step}) + 3.0 * stage
+                key = (when, [not offset[axis] for axis in order[stage + 1 :]])
+                if stage == depth - 1:
+                    key = (1e9, [])
+                events.append((key, part, stage, offset))
+    firsts.sort(key=lambda item: item[:2])
+    events.sort(key=lambda item: item[:3])
+    for _, part, offset in firsts:
+        send_of(part, parts[part][0], 0, offset).start()
+    for _, part, stage, offset in events:
+        order = parts[part][0]
+        before = dict(offset)
+        before[order[stage]] = 0
+        value = held(part, order, stage, before)[...].astype(jnp.float32)
+        for step in range(1, sizes[order[stage]]):
+            slot = slot_of(part, order, stage, step, offset)
+            arrived = recv_ref.at[part, slot]
             if stage == depth - 1:
-                where = pl.ds(parts[part][1], half)
-                out_ref[:, where] = (base_ref[:, where] + value).astype(out_ref.dtype)
-                continue
-            sum_ref[part, rank_at(sizes, order[1:], offset)] = value.astype(sum_ref.dtype)
-            flush()
-            if offset[order[stage + 1]]:
-                count = 1
-                for axis in order[stage + 1 :]:
-                    count *= sizes[axis]
-                slot_at[part] = begun[part] + (sizes[order[stage]] - 1) * count
-                waiting.append(send_of(part, order, stage + 1, offset))
-                slot_at[part] = begun[part]
+                flush()
+            pltpu.make_async_copy(arrived, arrived, recv_sem.at[part, slot]).wait()
+            value = value + arrived[...].astype(jnp.float32)
+        if stage == depth - 1:
+            where = pl.ds(parts[part][1], half)
+            out_ref[:, where] = (base_ref[:, where] + value).astype(out_ref.dtype)
+            continue
+        sum_ref[part, rank_at(sizes, order[1:], offset)] = value.astype(sum_ref.dtype)
         flush()
-        for part, (order, _, _) in enumerate(parts):
-            count = 1
-            for axis in order[stage + 1 :]:
-                count *= sizes[axis]
-            slot_at[part] = begun[part] + (sizes[order[stage]] - 1) * count
+        if offset[order[stage + 1]]:
+            waiting.append(send_of(part, order, stage + 1, offset))
     for part in range(len(parts)):
         sent = recv_ref.at[part]
         pltpu.make_async_copy(sent, sent, send_sem).wait()
@@ -309,7 +353,7 @@
             pltpu.SemaphoreType.DMA((len(parts), total)),
         ],
         compiler_params=pltpu.CompilerParams(
-            collective_id=collective_id, has_side_effects=True, vmem_limit_bytes=48 * 2**20
+            collective_id=collective_id, has_side_effects=True, vmem_limit_bytes=(3 * total) * rows * width * 2 + 4 * 2**20
         ),
     )(blocks, base)
 
@@ -359,8 +403,7 @@
 
     def gather_features(values, collective_id):
         parts = [("yc", 0, values.shape[1])]
-        blocks = gather_blocks(sizes, "yc", parts, values, collective_id)
-        return jnp.swapaxes(blocks, 0, 1).reshape(seq_rows, -1)
+        return gather_blocks(sizes, "yc", parts, values, collective_id, wide=True)
 
     full_resid = gather_features(residual, 0).astype(jnp.float32)
     normed = layer_norm(full_resid, in_gain).astype(jnp.bfloat16)
@@ -382,7 +425,7 @@
     parts = [("zxyc", 0, half), ("zyxc", half, sent.shape[1] - half)]
     got = gather_blocks(sizes, "zxyc", parts, sent, 2).reshape(-1, sent.shape[1])
 
-    rows = got[:, :width].reshape(ep_count, seq_rows, width)
+    rows = got.reshape(ep_count, seq_rows, -1)
     extra = got[:, width:].astype(jnp.float32)
     ids = extra[:, :top_count]
     parts = [extra[:, top_count * k : top_count * (k + 1)] for k in (1, 2, 3)]
@@ -400,7 +443,7 @@
     onehot = chosen.astype(jnp.bfloat16)
     slot_weight = jnp.sum(jnp.where(chosen, hit_weight[:, None, :], 0.0), axis=2)
     picked = jnp.einsum("gjr,grd->gjd", onehot, rows, preferred_element_type=jnp.float32)
-    picked = picked.astype(jnp.bfloat16).reshape(ep_count * capacity, width)
+    picked = picked.astype(jnp.bfloat16).reshape(ep_count * capacity, -1)[:, :width]
 
     def two_layers(values, gate_weight, up_weight, down_weight):
         gate_part = jnp.dot(values, gate_weight, preferred_element_type=jnp.float32)
@@ -416,7 +459,8 @@
         result.reshape(ep_count, capacity, width),
         preferred_element_type=jnp.float32,
     )
-    piece = lax.dynamic_slice_in_dim(rows, tp_place * per_dev, per_dev, 1).reshape(-1, width)
+    piece = lax.dynamic_slice_in_dim(rows, tp_place * per_dev, per_dev, 1)
+    piece = piece[:, :, :width].reshape(-1, width)
     gate_value = jax.nn.sigmoid(jnp.dot(piece, gate_vector, preferred_element_type=jnp.float32))
     shared = two_layers(piece, shared_gate, shared_up, shared_down) * gate_value[:, None]
     is_own = (jnp.arange(tp_count) == tp_place)[None, :, None, None]

time: 152 us -> 121 us (0.80)
  local copies, waits for them, and re-layouts: 22.8 us -> 12.9 us
  Pallas kernels: 83.5 us -> 75.4 us
  matrix products: 29 us -> 21.1 us
  other arithmetic: 14.1 us -> 10.2 us
    slice x4 -> x1, local copies, waits for them, and re-layouts: 11.1 us -> 1.3 us  [per_device(): piece = piece[:, :, :width].reshape(-1, width)]
    dot_general x5 -> x0, matrix products: 5.63 us -> none  [the longest x1 2.21 us: mixer_step(): input_im = jnp.einsum('tgh,gph->tgp', drive_f, push_im, precision=highest)]
    pallas_call x1, Pallas kernels: 33 us -> 27.7 us  [scatter_blocks(): pl.pallas_call(functools.partial(scatter_kernel, sizes, axes, parts), out...]
    pallas_call x3 -> x4, Pallas kernels: 50.4 us -> 47.7 us  [the longest x3 43.9 us: gather_blocks(): pl.pallas_call(functools.partial(gather_kernel, sizes, axes, parts, wide)...]
    dot_general x1, matrix products: 3.36 us -> 0.95 us  [per_device(): jnp.dot(own_rows(mixed_rows), out_weight, preferred_element_type=jnp.floa...]
    another operation x1, other arithmetic: 2.1 us -> 0.01 us  [mixer_step(): keep = jnp.stack([keep_re.reshape(-1), keep_im.reshape(-1)])]
    another operation x2, local copies, waits for them, and re-layouts: 2.22 us -> 0.16 us  [mixer_step(): keep = jnp.stack([keep_re.reshape(-1), keep_im.reshape(-1)])]
    reshape x1 -> x2, local copies, waits for them, and re-layouts: 0.1 us -> 2.11 us  [the longest x1 1.05 us: mixer_step(): jnp.stack([push_re, push_im]).transpose(0, 3, 1, 2)]
where the time goes in v2:
time: 121 us
  Pallas kernels  75.4 us (62%)
  matrix products  21.1 us (17%)
  local copies, waits for them, and re-layouts  12.9 us (11%)
  other arithmetic  10.2 us (8%)
    pallas_call x3, Pallas kernels, gather_blocks(): pl.pallas_call(functools.partial(gather_kernel, sizes, axes, parts, wide)...  43.9 us
    pallas_call x1, Pallas kernels, scatter_blocks(): pl.pallas_call(functools.partial(scatter_kernel, sizes, axes, parts), out...  27.7 us
    dot_general x2, matrix products, two_layers(): return jnp.dot(hidden, down_weight, preferred_element_type=jnp.float32)  9.42 us
    unnamed x34, local copies, waits for them, and re-layouts  4.82 us
    dot_general x2, matrix products, two_layers(): gate_part = jnp.dot(values, gate_weight, preferred_element_type=jnp.float32)  4.6 us
    pallas_call x1, Pallas kernels, mixer_step(): pl.pallas_call(mixer_kernel, out_shape=(jax.ShapeDtypeStruct((rows, chann...  3.77 us
    convert_element_type x1, other arithmetic, per_device(): total = total.astype(jnp.bfloat16).reshape(-1, per_dev, width)  3.18 us
    dot_general x1, matrix products, per_device(): jnp.einsum('gjr,grd->gjd', onehot, rows, preferred_element_type=jnp.float32)  3.15 us

profile of v2, /device:TPU:0, one launch (start us, length us, event | category | flops | bytes accessed | tf_op | source)
XLA Modules:
  0.0 120.5 jit_solution(1365914877341355992)
XLA Ops:
  0.6 0.0 copy-start
  0.7 0.8 exp.16
  1.5 0.1 broadcast_in_dim.73
  1.6 0.7 reduce_sum.67
  2.3 0.7 divide_multiply_fusion
  3.0 0.1 constant_dynamic-slice_fusion
  3.1 0.8 constant_dynamic-slice_fusion.1
  3.8 1.3 %reshape.94 = bf16[2048,1]{0,1:T(2,128)(2,1)} reshape(bf16[2048]{0:T(1024)(128)(2,1)} %param.33) | data formatting | bytes 8192 | tf_op args[12]
  5.1 0.1 copy.39
  5.2 0.6 convert_element_type.55
  5.8 0.1 copy.40
  5.9 0.6 subtract_convert_fusion
  6.5 0.8 add_divide_fusion
  7.4 0.1 stack_reshape.6
  7.4 0.1 stack_reshape.7
  7.5 1.0 multiply_subtract_fusion
  8.6 0.8 copy.35
  9.4 1.1 reshape.86.push_ref
  10.4 1.7 %copy.36 = f32[2,16,16,64]{3,2,1,0:T(8,128)} copy(f32[2,16,16,64]{3,1,2,0:T(8,128)} %bitcast.63) | data formatting | bytes 262144 | tf_op jit(solution)/shard_map/transpose | solution.py:93
  12.2 1.1 reshape.87.pull_ref
  13.2 8.3 %shard_map.212 = bf16[128,2048]{1,0:T(8,128)(2,1)S(1)} custom-call(bf16[128,512]{1,0:T(8,128)(2,1)S(1)} %copy-done.4), custom_call_target="tpu_custom_call" | custom-call | tf_op jit(solution)/shard_map/pallas_call | solution.py:229
  21.5 0.2 convert_reduce_fusion
  21.7 1.1 multiply_convert_fusion.normed_ref
  22.9 3.8 %shard_map.213 = (bf16[128,256]{1,0:T(8,128)(2,1)S(1)}, f32[2,128,1024]{2,1,0:T(8,128)}) custom-call(bf16[128,2048]{1,0:T(8,128)(2,1)S(1)} %multiply_convert_fusion.normed_ref, bf16[2048,256]{1,0:T(8,128)(2,1)S(1)} %copy-done.2, f32[2,128,1024]{2,1,0:T(8,128)S(1)} %copy-done.3, f32[2,1024]{1,0:T(2,128)S(1)} %pad_maximum_fusion.keep_ref, ...), custom_call_target="tpu_custom_call" | custom-call | tf_op jit(solution)/shard_map/pallas_call | solution.py:95
  26.6 5.3 %shard_map.214 = bf16[128,1024]{1,0:T(8,128)(2,1)S(1)} custom-call(bf16[128,256]{1,0:T(8,128)(2,1)S(1)} %get-tuple-element.4.in_ref), custom_call_target="tpu_custom_call" | custom-call | tf_op jit(solution)/shard_map/pallas_call | solution.py:229
  32.0 0.1 convert_element_type.52
  32.1 1.0 fusion.49
  33.1 0.1 multiply_convert_fusion.1
  33.3 0.1 concatenate.3.in_ref
  33.4 30.3 %shard_map.215 = bf16[32,32,2176]{2,1,0:T(8,128)(2,1)S(1)} custom-call(bf16[32,2176]{1,0:T(8,128)(2,1)S(1)} %concatenate.3.in_ref), custom_call_target="tpu_custom_call" | custom-call | tf_op jit(solution)/shard_map/pallas_call | solution.py:229
  63.7 2.0 %copy-done.1 = bf16[32,32,2176]{2,1,0:T(8,128)(2,1)} copy-done((bf16[32,32,2176]{2,1,0:T(8,128)(2,1)}, bf16[32,32,2176]{2,1,0:T(8,128)(2,1)S(1)}, u32[]{:S(2)}) %copy-start.1) | copy-done | bytes 4456472
  65.8 0.2 fusion.50
  66.0 0.6 fusion.21
  66.7 0.1 fusion.43
  66.8 0.1 select_reduce_fusion
  66.9 0.1 mul.210
  67.0 1.3 %constant_dynamic-slice_fusion.2 = bf16[8,32,2048]{2,1,0:T(8,128)(2,1)S(1)} fusion(bf16[8,128,2176]{2,1,0:T(8,128)(2,1)} %bitcast.52, s32[]{:T(128)S(6)} %select_n.20), kind=kLoop, calls=%fused_computation.69 | loop fusion | bytes 2097156 | tf_op jit(solution)/shard_map/slice | solution.py:463
  68.3 3.1 %convolution_convert_fusion = bf16[8,32,2176]{2,1,0:T(8,128)(2,1)S(1)} fusion(bf16[8,128,2176]{2,1,0:T(8,128)(2,1)} %bitcast.53, f32[8,128]{1,0:T(8,128)S(1)} %fusion.43, pred[8,128]{1,0:T(8,128)(4,1)S(1)} %bitcast.66), kind=kOutput, calls=%fused_computation.3 | convolution fusion | flops 143228928 | bytes 5575680 | tf_op jit(solution)/shard_map/gjr,grd->gjd/dot_general | solution.py:445
  71.5 0.4 fusion.52
  71.9 0.6 copy-done.7
  72.5 1.5 %fusion.6 = f32[256,512]{1,0:T(8,128)} fusion(bf16[1,2048,512]{2,1,0:T(8,128)(2,1)S(1)} %copy-done.14, bf16[256,2176]{1,0:T(8,128)(2,1)S(1)} %bitcast.60), kind=kOutput, calls=%fused_computation.11 | convolution fusion | flops 536870912 | bytes 3670016 | tf_op jit(solution)/shard_map/dot_general | solution.py:449
  74.0 4.3 %fusion.2 = bf16[256,2048]{1,0:T(8,128)(2,1)} fusion(bf16[1,512,2048]{2,1,0:T(8,128)(2,1)S(1)} %copy-done, f32[256]{0:T(256)S(1)} %mul.210, bf16[1,2048,512]{2,1,0:T(8,128)(2,1)} %param.37, bf16[256,2176]{1,0:T(8,128)(2,1)} %bitcast.61, f32[256,512]{1,0:T(8,128)} %fusion.6), kind=kOutput, calls=%fused_computation.6 | convolution fusion | flops 1075576832 | bytes 6816768 | tf_op jit(solution)/shard_map/dot_general | solution.py:452
  78.3 3.1 %fusion.51 = f32[256,512]{1,0:T(8,128)} fusion(bf16[256,2048]{1,0:T(8,128)(2,1)S(1)} %bitcast.57, bf16[2048,512]{1,0:T(8,128)(2,1)} %param.39), kind=kOutput, calls=%fused_computation.82 | convolution fusion | flops 536870912 | bytes 3670016 | tf_op jit(solution)/shard_map/dot_general | solution.py:449
  81.4 5.1 %convolution_multiply_fusion = f32[256,2048]{1,0:T(8,128)} fusion(bf16[512,2048]{1,0:T(8,128)(2,1)} %param.41, bf16[256,2048]{1,0:T(8,128)(2,1)S(1)} %bitcast.58, bf16[2048,512]{1,0:T(8,128)(2,1)} %param.40, f32[256]{0:T(256)S(1)} %add_divide_fusion.1, f32[256,512]{1,0:T(8,128)} %fusion.51), kind=kOutput, calls=%fused_computation.4 | convolution fusion | flops 1075052544 | bytes 7865344 | tf_op jit(solution)/shard_map/dot_general | solution.py:452
  86.5 2.5 %fusion.35 = f32[8,128,2048]{2,1,0:T(8,128)S(1)} fusion(bf16[8,32,2048]{2,1,0:T(8,128)(2,1)} %bitcast.62, f32[8,128]{1,0:T(8,128)S(1)} %fusion.43, pred[8,128]{1,0:T(8,128)(4,1)S(1)} %bitcast.67), kind=kOutput, calls=%fused_computation.48 | convolution fusion | flops 134283264 | bytes 9442304 | tf_op jit(solution)/shard_map/gjr,gjd->grd/dot_general | solution.py:456
  89.0 3.2 %fusion.1.in_ref = bf16[32,32,2048]{2,1,0:T(8,128)(2,1)S(1)} fusion(f32[32,32,2048]{2,1,0:T(8,128)S(1)} %bitcast.55, f32[8,32,2048]{2,1,0:T(8,128)} %bitcast.59, pred[32]{0:T(512)(128)(4,1)S(1)} %broadcast_in_dim.73), kind=kLoop, calls=%fused_computation.2 | loop fusion | flops 6291456 | bytes 14680096 | tf_op jit(solution)/shard_map/convert_element_type | solution.py:470
  92.2 27.7 %shard_map.216 = bf16[32,2048]{1,0:T(8,128)(2,1)S(1)} custom-call(bf16[32,32,2048]{2,1,0:T(8,128)(2,1)S(1)} %fusion.1.in_ref, f32[32,2048]{1,0:T(8,128)S(1)} %get-tuple-element.25.base_ref), custom_call_target="tpu_custom_call" | custom-call | tf_op jit(solution)/shard_map/pallas_call | solution.py:344
  119.9 0.7 copy.42
  (36 shorter events, 0.2 us)
Async XLA Ops:
  0.6 73.3 %copy-start = (bf16[1,512,2048]{2,1,0:T(8,128)(2,1)S(1)}, bf16[1,512,2048]{2,1,0:T(8,128)(2,1)}, u32[]{:S(2)}) copy-start(bf16[1,512,2048]{2,1,0:T(8,128)(2,1)} %param.38) | copy-start | bytes 6291460
  0.6 12.6 %copy-start.4 = (bf16[128,512]{1,0:T(8,128)(2,1)S(1)}, bf16[128,512]{1,0:T(8,128)(2,1)}, u32[]{:S(2)}) copy-start(bf16[128,512]{1,0:T(8,128)(2,1)} %in_ref.1) | copy-start | bytes 393220
  8.6 14.3 %copy-start.2 = (bf16[2048,256]{1,0:T(8,128)(2,1)S(1)}, bf16[2048,256]{1,0:T(8,128)(2,1)}, u32[]{:S(2)}) copy-start(bf16[2048,256]{1,0:T(8,128)(2,1)} %in_weight_ref.1) | copy-start | bytes 3145732
  8.6 14.3 %copy-start.5 = (f32[256]{0:T(256)S(1)}, f32[256]{0:T(256)}, u32[]{:S(2)}) copy-start(f32[256]{0:T(256)} %param.30) | copy-start | bytes 3076
  13.2 9.6 %copy-start.3 = (f32[2,128,1024]{2,1,0:T(8,128)S(1)}, f32[2,128,1024]{2,1,0:T(8,128)}, u32[]{:S(2)}) copy-start(f32[2,128,1024]{2,1,0:T(8,128)} %state_ref.1) | copy-start | bytes 3145732
  22.9 9.2 %copy-start.6 = (bf16[1024,2048]{1,0:T(8,128)(2,1)S(1)}, bf16[1024,2048]{1,0:T(8,128)(2,1)}, u32[]{:S(2)}) copy-start(bf16[1024,2048]{1,0:T(8,128)(2,1)} %param.31) | copy-start | bytes 12582916
  32.1 1.0 copy-start.13
  32.1 1.1 copy-start.9
  32.1 1.1 copy-start.10
  32.1 1.1 copy-start.11
  32.1 1.1 copy-start.12
  63.7 2.0 %copy-start.1 = (bf16[32,32,2176]{2,1,0:T(8,128)(2,1)}, bf16[32,32,2176]{2,1,0:T(8,128)(2,1)S(1)}, u32[]{:S(2)}) copy-start(bf16[32,32,2176]{2,1,0:T(8,128)(2,1)S(1)} %shard_map.215) | copy-start | bytes 13369348
  68.3 3.2 %copy-start.8 = (bf16[2048,1]{0,1:T(2,128)(2,1)S(1)}, bf16[2048,1]{0,1:T(2,128)(2,1)}, u32[]{:S(2)}) copy-start(bf16[2048,1]{0,1:T(2,128)(2,1)} %reshape.94) | copy-start | bytes 12292
  68.3 4.2 %copy-start.14 = (bf16[1,2048,512]{2,1,0:T(8,128)(2,1)S(1)}, bf16[1,2048,512]{2,1,0:T(8,128)(2,1)}, u32[]{:S(2)}) copy-start(bf16[1,2048,512]{2,1,0:T(8,128)(2,1)} %param.36) | copy-start | bytes 6291460
  71.5 1.0 copy-start.7
